TPU v7x, 32 devices: a whole 2x2x4 slice. The times are simulated.
32 devices in a mesh: fs: 8 (over z, y), tp: 4 (over x, core).
Axes of the slice: x: 2, y: 2, z: 4, core: 2. Of those that a mesh axis runs over, the one named last changes fastest.
Arguments:
- saved_inputs: bfloat16 [4096, 3072], P('fs'), may hold values from -6 to 6
- query_cotangent: bfloat16 [4096, 3072], P('fs', 'tp'), may hold values from -0.75 to 0.75
- attn_outputs: bfloat16 [4096, 3072], P('fs', 'tp'), may hold values from -6 to 6
- out_cotangent: bfloat16 [4096, 3072], P('fs'), may hold values from -0.75 to 0.75
- left_factor: bfloat16 [3072, 384], P('fs', 'tp'), may hold values from -0.109375 to 0.109375
- right_factor: bfloat16 [3072, 384], P('fs', 'tp'), may hold values from -0.109375 to 0.109375
- query_master: float32 [3072, 3072], P('fs', 'tp'), may hold values from -0.109375 to 0.109375
- out_master: float32 [3072, 3072], P('tp', 'fs'), may hold values from -0.109375 to 0.109375
- first_moment: float32 [2, 384, 3072], P(None, 'fs', 'tp'), may hold values from -14 to 14
- second_moment: float32 [2, 384, 3072], P(None, 'fs', 'tp'), may hold values from 0.3 to 3
Outputs:
- query_new: float32 [3072, 3072], P('fs', 'tp')
- out_new: float32 [3072, 3072], P('tp', 'fs')
- query_copy: bfloat16 [3072, 3072], P(None, 'tp')
- out_copy: bfloat16 [3072, 3072], P('tp')
- first_new: float32 [2, 384, 3072], P(None, 'fs', 'tp')
- second_new: float32 [2, 384, 3072], P(None, 'fs', 'tp')
All inputs are finite; a program needn't handle non-finite values.
Results may differ from a plain program's by a relative error of at most 0.0025.
Values may be sent and summed in bfloat16 or wider, within the bound.
A program may use at most 64 MiB of HBM per device.

v0:
```python
import functools

import jax
import jax.numpy as jnp
from jax import lax
from jax.experimental import pallas as pl
from jax.experimental.pallas import tpu as pltpu
from jax.sharding import PartitionSpec as P

MESH = pl.DeviceIdType.MESH
PAIR = 2
NT = (((1,), (1,)), ((), ()))
TN = (((0,), (0,)), ((), ()))


def moment_step(first, second, grads):
    first_next = 0.9 * first + 0.1 * grads
    second_next = 0.99 * second + 0.01 * grads * grads
    return (first_next, second_next, first_next / (jnp.sqrt(second_next) + 1e-08))


def rows(index, size):
    return pl.ds(pl.multiple_of(index * size, size), size)


def peer_along(axis, index):
    if axis == "fs":
        return (index, lax.axis_index("tp"))
    return (lax.axis_index("fs"), index)


class Gather:
    def __init__(self, axis, count, view, sems, own=None):
        self.axis, self.outer, self.view, self.sems = axis, count // PAIR, view, sems
        me = lax.axis_index(axis)
        self.high, self.low = me // PAIR, lax.rem(me, PAIR)
        self.own = view(me) if own is None else own
        self.me = me

    def copy(self, src, dst, stage, slot, target):
        return pltpu.make_async_remote_copy(
            src_ref=src,
            dst_ref=dst,
            send_sem=self.sems.at[stage, 0, slot],
            recv_sem=self.sems.at[stage, 1, slot],
            device_id=peer_along(self.axis, target),
            device_id_type=MESH,
        )

    def index(self, offset, low):
        return lax.rem(self.high + offset, self.outer) * PAIR + low

    def outward(self, offset):
        return self.copy(self.own, self.view(self.me), 0, offset, self.index(offset, self.low))

    def inward(self, offset):
        source = self.index(self.outer - offset, self.low)
        src = self.own if offset == 0 else self.view(source)
        partner = self.high * PAIR + 1 - self.low
        return self.copy(src, self.view(self.me if offset == 0 else source), 1, offset, partner)

    def start_outward(self):
        for offset in range(self.outer - 1, 0, -1):
            self.outward(offset).start()

    def start_inward(self):
        self.inward(0).start()

    def start(self):
        self.start_outward()
        self.start_inward()

    def forward(self):
        for offset in range(self.outer - 1, 0, -1):
            self.outward(offset).wait_recv()
            self.inward(offset).start()

    def finish(self):
        for offset in range(self.outer):
            self.inward(offset).wait_recv()
        for offset in range(1, self.outer):
            self.outward(offset).wait_send()
        for offset in range(self.outer):
            self.inward(offset).wait_send()


def kernel(
    n_fs,
    n_tp,
    saved_hbm,
    outcot_hbm,
    querycot_hbm,
    attn_hbm,
    query_hbm,
    out_hbm,
    factor_ref,
    first_ref,
    second_ref,
    query_out,
    out_out,
    query_copy,
    out_copy,
    first_out,
    second_out,
    factors_ref,
    dirs_ref,
    query_master,
    out_master,
    query_early,
    out_early,
    saved,
    outcot,
    querycot,
    attn,
    proj,
    grad,
    pair_send,
    pair_recv,
    far_send,
    far_recv,
    own_dir,
    square_buf,
    load_sems,
    factor_sems,
    proj_sems,
    columns_sems,
    pair_sems,
    far_sems,
    dir_sems,
    square_sems,
    early_sems,
    late_sems,
):
    me, column = lax.axis_index("fs"), lax.axis_index("tp")
    high, low = me // PAIR, lax.rem(me, PAIR)
    outer = n_fs // PAIR
    part = factor_ref.shape[1]
    width = factor_ref.shape[2]
    depth = first_ref.shape[1]
    loads = [
        pltpu.make_async_copy(src, dst, load_sems.at[i])
        for i, (src, dst) in enumerate(
            (
                (saved_hbm, saved),
                (outcot_hbm, outcot),
                (querycot_hbm, querycot),
                (attn_hbm, attn),
                (query_hbm, query_master),
                (out_hbm, out_master),
            )
        )
    ]
    for load in loads[4:] + loads[:4]:
        load.start()

    peers = [(lax.rem(high + i, outer) * PAIR + low, column) for i in range(1, outer)]
    peers.append((high * PAIR + 1 - low, column))
    peers += [(me, lax.rem(column + i, n_tp)) for i in range(1, n_tp)]
    barrier = pltpu.get_barrier_semaphore()
    for peer in peers:
        pl.semaphore_signal(barrier, inc=1, device_id=peer, device_id_type=MESH)
    pl.semaphore_wait(barrier, len(peers))

    factors = Gather(
        "fs",
        n_fs,
        lambda i: factors_ref.at[:, rows(column, part), rows(i, width)],
        factor_sems,
        own=factor_ref,
    )
    factors.start()
    factors_ref[:, rows(column, part), rows(me, width)] = factor_ref[...]

    half = query_copy.shape[1] // 2
    early = (
        Gather("fs", n_fs, lambda i: query_copy.at[rows(i, width), :half], early_sems.at[0], own=query_early),
        Gather("fs", n_fs, lambda i: out_copy.at[:half, rows(i, width)], early_sems.at[1], own=out_early),
    )
    loads[4].wait()
    query_early[...] = query_master[:, :half].astype(query_early.dtype)
    loads[5].wait()
    out_early[...] = out_master[:half, :].astype(out_early.dtype)
    for gather in early:
        gather.start_outward()
    factors.forward()
    for gather in early:
        gather.start_inward()
    factors.finish()

    gathers = []
    for k, tokens in enumerate((saved, outcot)):
        loads[k].wait()
        part_proj = lax.dot_general(
            factors_ref[k, rows(column, part), :],
            tokens[...],
            NT,
            preferred_element_type=jnp.float32,
        )
        proj[k, rows(column, part), :] = part_proj.astype(proj.dtype)
        gather = Gather(
            "tp", n_tp, lambda i, k=k: proj.at[k, rows(i, part), :], proj_sems.at[k]
        )
        gather.start()
        gathers.append(gather)
    columns = Gather("tp", n_tp, lambda i: factors_ref.at[:, rows(i, part), :], columns_sems)
    for gather in gathers:
        gather.forward()
    columns.start()
    for k, (gather, cot) in enumerate(zip(gathers, (querycot, attn))):
        gather.finish()
        loads[2 + k].wait()
        grad[k, :, :] = jnp.dot(proj[k], cot[...], preferred_element_type=jnp.float32)

    def pair_copy(offset):
        return pltpu.make_async_remote_copy(
            src_ref=pair_send.at[offset],
            dst_ref=pair_recv.at[offset],
            send_sem=pair_sems.at[0, offset],
            recv_sem=pair_sems.at[1, offset],
            device_id=(high * PAIR + 1 - low, column),
            device_id_type=MESH,
        )

    def far_copy(offset):
        return pltpu.make_async_remote_copy(
            src_ref=far_send.at[offset],
            dst_ref=far_recv.at[offset],
            send_sem=far_sems.at[0, offset],
            recv_sem=far_sems.at[1, offset],
            device_id=(lax.rem(high + offset, outer) * PAIR + low, column),
            device_id_type=MESH,
        )

    order = list(range(outer - 1, 0, -1)) + [0]
    for offset in order:
        target = lax.rem(high + offset, outer) * PAIR + 1 - low
        pair_send[offset] = grad[:, rows(target, depth), :].astype(pair_send.dtype)
        pair_copy(offset).start()
    for offset in order:
        target = lax.rem(high + offset, outer) * PAIR + low
        pair_copy(offset).wait_recv()
        both = grad[:, rows(target, depth), :] + pair_recv[offset].astype(jnp.float32)
        if offset:
            far_send[offset] = both.astype(far_send.dtype)
            far_copy(offset).start()
    total = both
    columns.forward()
    for gather in early:
        gather.forward()
    for offset in range(1, outer):
        far_copy(offset).wait_recv()
        total = total + far_recv[offset].astype(jnp.float32)

    first_new, second_new, direction = moment_step(first_ref[...], second_ref[...], total)
    own_dir[...] = direction.astype(own_dir.dtype)
    spread = Gather("fs", n_fs, lambda i: dirs_ref.at[:, rows(i, depth), :], dir_sems, own=own_dir)
    spread.start()
    dirs_ref[:, rows(me, depth), :] = own_dir[...]
    first_out[...] = first_new
    second_out[...] = second_new
    squares = direction * direction
    shape = square_buf.shape[1:]
    row = lax.broadcasted_iota(jnp.int32, shape, 0)
    mine = jnp.where(row == 0, jnp.sum(squares[0]), jnp.sum(squares[1]))

    rounds = (
        [(me, lax.rem(column + i, n_tp)) for i in range(1, n_tp)],
        [(lax.rem(high + i, outer) * PAIR + low, column) for i in range(1, outer)],
        [(high * PAIR + 1 - low, column)],
    )
    slot = 0
    tiny = []
    for stage, targets in enumerate(rounds):
        square_buf[slot] = mine
        base = slot
        copies = []
        for target in targets:
            slot += 1
            copies.append(
                pltpu.make_async_remote_copy(
                    src_ref=square_buf.at[base],
                    dst_ref=square_buf.at[slot],
                    send_sem=square_sems.at[0, slot],
                    recv_sem=square_sems.at[1, slot],
                    device_id=target,
                    device_id_type=MESH,
                )
            )
        for copy in copies:
            copy.start()
        if stage == 1:
            spread.forward()
        for i, copy in enumerate(copies):
            copy.wait_recv()
            mine = mine + square_buf[base + 1 + i]
        tiny += copies
        slot += 1
    spread.finish()
    columns.finish()

    entries = dirs_ref.shape[1] * dirs_ref.shape[2] * n_tp
    scale = 0.01 * lax.rsqrt(mine / entries + 1e-06)
    query_scale, out_scale = scale[0:1, 0:1], scale[1:2, 0:1]

    def step(k, block, part_of_features):
        factor = factors_ref[k, :, rows(block, width)]
        direction = dirs_ref[k, :, part_of_features]
        pair = (factor, direction) if k == 0 else (direction, factor)
        return lax.dot_general(*pair, TN, preferred_element_type=jnp.float32)

    tall, deep = width // 2, half // 2
    late_query = [
        Gather("fs", n_fs, lambda i, p=p: query_copy.at[rows(2 * i + p, tall), half:], late_sems.at[p])
        for p in range(2)
    ]
    late_out = [
        Gather(
            "fs",
            n_fs,
            lambda i, p=p: out_copy.at[half + p * deep : half + (p + 1) * deep, rows(i, width)],
            late_sems.at[2 + p],
        )
        for p in range(2)
    ]
    late = late_query + late_out
    for part_of_features in (slice(half, None), slice(0, half)):
        query_new = query_master[:, part_of_features] - query_scale * step(0, me, part_of_features)
        query_out[:, part_of_features] = query_new
        query_copy[rows(me, width), part_of_features] = query_new.astype(query_copy.dtype)
        if part_of_features.start:
            for gather in late_query:
                gather.start()
        out_new = out_master[part_of_features, :] - out_scale * step(1, me, part_of_features)
        out_out[part_of_features, :] = out_new
        out_copy[part_of_features, rows(me, width)] = out_new.astype(out_copy.dtype)
        if part_of_features.start:
            for gather in late_out:
                gather.start()
    for gather in early:
        gather.finish()

    def finish_block(i, carry):
        block = lax.rem(me + i, n_fs)
        where = rows(block, width)
        query = query_copy[where, :half].astype(jnp.float32)
        query_copy[where, :half] = (query - query_scale * step(0, block, slice(0, half))).astype(query_copy.dtype)
        out = out_copy[:half, where].astype(jnp.float32)
        out_copy[:half, where] = (out - out_scale * step(1, block, slice(0, half))).astype(out_copy.dtype)
        return carry

    lax.fori_loop(1, n_fs, finish_block, 0)
    for gather in late:
        gather.forward()
    for gather in late:
        gather.finish()
    for offset in order:
        pair_copy(offset).wait_send()
        if offset:
            far_copy(offset).wait_send()
    for copy in tiny:
        copy.wait_send()


def fast_body(
    n_fs,
    n_tp,
    saved_inputs,
    query_cotangent,
    attn_outputs,
    out_cotangent,
    left_factor,
    right_factor,
    query_master,
    out_master,
    first_moment,
    second_moment,
):
    tokens, model = saved_inputs.shape
    features = query_cotangent.shape[1]
    width, part = left_factor.shape
    depth = first_moment.shape[1]
    rank = part * n_tp
    outer = n_fs // PAIR
    half = features // 2
    low, wide = jnp.bfloat16, jnp.float32
    vmem = pl.BlockSpec(memory_space=pltpu.VMEM)
    anywhere = pl.BlockSpec(memory_space=pl.ANY)
    dma = pltpu.SemaphoreType.DMA
    tiny_slots = n_tp + outer + PAIR
    factor = jnp.stack([left_factor.T, right_factor.T])
    return pl.pallas_call(
        functools.partial(kernel, n_fs, n_tp),
        out_shape=(
            jax.ShapeDtypeStruct((width, features), wide),
            jax.ShapeDtypeStruct((features, width), wide),
            jax.ShapeDtypeStruct((model, features), low),
            jax.ShapeDtypeStruct((features, model), low),
            jax.ShapeDtypeStruct(first_moment.shape, wide),
            jax.ShapeDtypeStruct(first_moment.shape, wide),
        ),
        in_specs=[anywhere] * 6 + [vmem] * 3,
        out_specs=(vmem,) * 6,
        scratch_shapes=[
            pltpu.VMEM((2, rank, model), low),
            pltpu.VMEM((2, rank, features), low),
            pltpu.VMEM((width, features), wide),
            pltpu.VMEM((features, width), wide),
            pltpu.VMEM((width, half), low),
            pltpu.VMEM((half, width), low),
            pltpu.VMEM((tokens, model), low),
            pltpu.VMEM((tokens, model), low),
            pltpu.VMEM((tokens, features), low),
            pltpu.VMEM((tokens, features), low),
            pltpu.VMEM((2, rank, tokens), low),
            pltpu.VMEM((2, rank, features), wide),
            pltpu.VMEM((outer, 2, depth, features), low),
            pltpu.VMEM((outer, 2, depth, features), low),
            pltpu.VMEM((outer, 2, depth, features), low),
            pltpu.VMEM((outer, 2, depth, features), low),
            pltpu.VMEM((2, depth, features), low),
            pltpu.VMEM((tiny_slots, 8, 128), wide),
            dma((6,)),
            dma((2, 2, outer)),
            dma((2, 2, 2, n_tp // PAIR)),
            dma((2, 2, n_tp // PAIR)),
            dma((2, outer)),
            dma((2, outer)),
            dma((2, 2, outer)),
            dma((2, tiny_slots)),
            dma((2, 2, 2, outer)),
            dma((4, 2, 2, outer)),
        ],
        compiler_params=pltpu.CompilerParams(
            collective_id=0, has_side_effects=True, vmem_limit_bytes=56 * 2**20
        ),
        cost_estimate=pl.CostEstimate(
            flops=4 * tokens * rank * (model + features), bytes_accessed=200 * 2**20, transcendentals=0
        ),
    )(
        saved_inputs,
        out_cotangent,
        query_cotangent,
        attn_outputs,
        query_master,
        out_master,
        factor,
        first_moment,
        second_moment,
    )


def plain_body(
    saved_inputs,
    query_cotangent,
    attn_outputs,
    out_cotangent,
    left_factor,
    right_factor,
    query_master,
    out_master,
    first_moment,
    second_moment,
):
    left_part = jnp.dot(
        saved_inputs,
        lax.all_gather(left_factor, "fs", axis=0, tiled=True),
        preferred_element_type=jnp.float32,
    )
    right_part = jnp.dot(
        out_cotangent,
        lax.all_gather(right_factor, "fs", axis=0, tiled=True),
        preferred_element_type=jnp.float32,
    )
    left_proj, right_proj, left_rows, right_rows = (
        lax.all_gather(left_part.astype(jnp.bfloat16), "tp", axis=1, tiled=True),
        lax.all_gather(right_part.astype(jnp.bfloat16), "tp", axis=1, tiled=True),
        lax.all_gather(left_factor, "tp", axis=1, tiled=True),
        lax.all_gather(right_factor, "tp", axis=1, tiled=True),
    )
    depth = first_moment.shape[1]
    grad_query = lax.dot_general(left_proj, query_cotangent, TN, preferred_element_type=jnp.float32)
    grad_output = lax.dot_general(right_proj, attn_outputs, TN, preferred_element_type=jnp.float32)
    summed = lax.psum_scatter(
        jnp.stack([grad_query, grad_output], axis=1), "fs", scatter_dimension=0, tiled=True
    )
    grads = jnp.transpose(summed, (1, 0, 2))
    first_new, second_new, own_direction = moment_step(first_moment, second_moment, grads)
    direction_all = lax.all_gather(own_direction.astype(jnp.bfloat16), "fs", axis=1, tiled=True)
    squares = jnp.sum(own_direction * own_direction, axis=(1, 2))
    total = lax.psum(squares, ("fs", "tp"))
    entries = depth * lax.axis_size("fs") * own_direction.shape[2] * lax.axis_size("tp")
    scale = lax.rsqrt(total / entries + 1e-06)
    step_query = scale[0] * jnp.dot(left_rows, direction_all[0], preferred_element_type=jnp.float32)
    step_output = scale[1] * lax.dot_general(
        direction_all[1], right_rows, (((0,), (1,)), ((), ())), preferred_element_type=jnp.float32
    )
    query_new = query_master - 0.01 * step_query
    out_new = out_master - 0.01 * step_output
    query_copy, out_copy = (
        lax.all_gather(query_new.astype(jnp.bfloat16), "fs", axis=0, tiled=True),
        lax.all_gather(out_new.astype(jnp.bfloat16), "fs", axis=1, tiled=True),
    )
    return (query_new, out_new, query_copy, out_copy, first_new, second_new)


def choose_body(n_fs, n_tp, *args):
    left_factor, first_moment = args[4], args[8]
    model, part = args[0].shape[1], left_factor.shape[1]
    aligned = part % 16 == 0 and first_moment.shape[1] % 16 == 0
    aligned = aligned and model // n_fs % 128 == 0 and first_moment.shape[2] % 256 == 0
    aligned = aligned and model // n_fs % 32 == 0 and first_moment.shape[2] % 64 == 0
    if aligned and n_fs % PAIR == 0 and n_tp % PAIR == 0:
        return fast_body(n_fs, n_tp, *args)
    return plain_body(*args)


def solution(mesh):
    return jax.shard_map(
        functools.partial(choose_body, mesh.shape["fs"], mesh.shape["tp"]),
        mesh=mesh,
        in_specs=(
            P("fs", None),
            P("fs", "tp"),
            P("fs", "tp"),
            P("fs", None),
            P("fs", "tp"),
            P("fs", "tp"),
            P("fs", "tp"),
            P("tp", "fs"),
            P(None, "fs", "tp"),
            P(None, "fs", "tp"),
        ),
        out_specs=(
            P("fs", "tp"),
            P("tp", "fs"),
            P(None, "tp"),
            P("tp", None),
            P(None, "fs", "tp"),
            P(None, "fs", "tp"),
        ),
        check_vma=False,
    )
```

profile of v0, /device:TPU:0, one launch (start us, length us, event | category | flops | bytes accessed | tf_op | source)
XLA Modules:
  0.0 194.7 jit_solution(6283920057721334857)
XLA Ops:
  0.6 1.6 pad_maximum_fusion.factor_ref
  2.2 181.6 %shard_map.145 = (f32[384,768]{1,0:T(8,128)}, f32[768,384]{1,0:T(8,128)}, bf16[3072,768]{1,0:T(8,128)(2,1)}, bf16[768,3072]{1,0:T(8,128)(2,1)}, f32[2,48,768]{2,1,0:T(8,128)}, /*index=5*/f32[2,48,768]{2,1,0:T(8,128)}) custom-call(bf16[512,3072]{1,0:T(8,128)(2,1)} %saved_hbm.1, bf16[512,3072]{1,0:T(8,128)(2,1)} %outcot_hbm.1, bf16[512,768]{1,0:T(8,128)(2,1)} %querycot_hbm.1, ...), custom_call_target="tpu_custom_call" | custom-call | flops 3019898880 | bytes 209715200 | tf_op jit(solution)/shard_map/pallas_call | solution.py:391
  183.9 0.0 copy-start
  183.9 2.5 %copy.22 = f32[384,768]{1,0:T(8,128)} copy(f32[384,768]{1,0:T(8,128)} %get-tuple-element.12) | data formatting | bytes 2359296
  186.4 0.0 slice-start
  186.4 2.5 %copy.23 = f32[768,384]{1,0:T(8,128)} copy(f32[768,384]{1,0:T(8,128)} %get-tuple-element.13) | data formatting | bytes 2359296
  188.9 0.0 copy-done
  188.9 0.0 slice-start.1
  188.9 2.2 %copy.24 = bf16[3072,768]{1,0:T(8,128)(2,1)} copy(bf16[3072,768]{1,0:T(8,128)(2,1)S(1)} %copy-done) | data formatting | bytes 9437184
  191.1 0.0 slice-done
  191.1 0.0 slice-done.1
  191.1 0.0 copy-start.2
  191.1 0.0 copy-start.1
  191.1 2.2 %copy.25 = bf16[768,3072]{1,0:T(8,128)(2,1)} copy(bf16[768,3072]{1,0:T(8,128)(2,1)S(1)} %bitcast.7) | data formatting | bytes 9437184
  193.3 0.0 copy-done.2
  193.3 0.7 copy.26
  194.0 0.0 copy-done.1
  194.0 0.7 copy.27
  (1 shorter events, 0.0 us)
Async XLA Ops:
  183.9 5.0 %copy-start = (bf16[3072,768]{1,0:T(8,128)(2,1)S(1)}, bf16[3072,768]{1,0:T(8,128)(2,1)}, u32[]{:S(2)}) copy-start(bf16[3072,768]{1,0:T(8,128)(2,1)} %get-tuple-element.14) | copy-start | bytes 14155780
  186.4 4.7 %slice-start = ((s8[4718592]{0:T(1024)(128)(4,1)}), s8[4194304]{0:T(1024)(128)(4,1)S(1)}, s32[]{:S(2)}) async-start(s8[4718592]{0:T(1024)(128)(4,1)} %bitcast.6), calls=%async_computation | async-start | bytes 8388608
  188.9 2.2 %slice-start.1 = ((s8[4718592]{0:T(1024)(128)(4,1)}), s8[524288]{0:T(1024)(128)(4,1)S(1)}, s32[]{:S(2)}) async-start(s8[4718592]{0:T(1024)(128)(4,1)} %bitcast.6), calls=%async_computation.1 | async-start | bytes 1048576
  191.1 2.2 %copy-start.2 = (f32[2,48,768]{2,1,0:T(8,128)S(1)}, f32[2,48,768]{2,1,0:T(8,128)}, u32[]{:S(2)}) copy-start(f32[2,48,768]{2,1,0:T(8,128)} %get-tuple-element.16) | copy-start | bytes 884740
  191.1 2.9 %copy-start.1 = (f32[2,48,768]{2,1,0:T(8,128)S(1)}, f32[2,48,768]{2,1,0:T(8,128)}, u32[]{:S(2)}) copy-start(f32[2,48,768]{2,1,0:T(8,128)} %get-tuple-element.17) | copy-start | bytes 884740
where the time goes:
time: 195 us
  Pallas kernels  182 us (93%)
  local copies, waits for them, and re-layouts  10.8 us (6%)
    pallas_call x1, Pallas kernels, fast_body(): pl.pallas_call(functools.partial(kernel, n_fs, n_tp), out_shape=(jax.Shap...  182 us
    unnamed x16, local copies, waits for them, and re-layouts  10.8 us

commit v1 on v0

--- a/solution.py
+++ b/solution.py
@@ -361,6 +361,16 @@
         copy.wait_send()
 
 
+def store_kernel(*refs):
+    count = len(refs) // 2
+    sems = refs[-1]
+    copies = [pltpu.make_async_copy(refs[i], refs[count + i], sems.at[i]) for i in range(count)]
+    for copy in copies:
+        copy.start()
+    for copy in copies:
+        copy.wait()
+
+
 def fast_body(
     n_fs,
     n_tp,
@@ -388,15 +398,15 @@
     dma = pltpu.SemaphoreType.DMA
     tiny_slots = n_tp + outer + PAIR
     factor = jnp.stack([left_factor.T, right_factor.T])
-    return pl.pallas_call(
+    results = pl.pallas_call(
         functools.partial(kernel, n_fs, n_tp),
         out_shape=(
-            jax.ShapeDtypeStruct((width, features), wide),
-            jax.ShapeDtypeStruct((features, width), wide),
-            jax.ShapeDtypeStruct((model, features), low),
-            jax.ShapeDtypeStruct((features, model), low),
-            jax.ShapeDtypeStruct(first_moment.shape, wide),
-            jax.ShapeDtypeStruct(first_moment.shape, wide),
+            pltpu.VMEM((width, features), wide),
+            pltpu.VMEM((features, width), wide),
+            pltpu.VMEM((model, features), low),
+            pltpu.VMEM((features, model), low),
+            pltpu.VMEM(first_moment.shape, wide),
+            pltpu.VMEM(first_moment.shape, wide),
         ),
         in_specs=[anywhere] * 6 + [vmem] * 3,
         out_specs=(vmem,) * 6,
@@ -431,7 +441,7 @@
             dma((4, 2, 2, outer)),
         ],
         compiler_params=pltpu.CompilerParams(
-            collective_id=0, has_side_effects=True, vmem_limit_bytes=56 * 2**20
+            collective_id=0, has_side_effects=True, vmem_limit_bytes=46 * 2**20
         ),
         cost_estimate=pl.CostEstimate(
             flops=4 * tokens * rank * (model + features), bytes_accessed=200 * 2**20, transcendentals=0
@@ -447,6 +457,15 @@
         first_moment,
         second_moment,
     )
+    return pl.pallas_call(
+        store_kernel,
+        out_shape=tuple(jax.ShapeDtypeStruct(r.shape, r.dtype) for r in results),
+        in_specs=[vmem] * len(results),
+        out_specs=(anywhere,) * len(results),
+        scratch_shapes=[dma((len(results),))],
+        compiler_params=pltpu.CompilerParams(vmem_limit_bytes=2**20),
+        cost_estimate=pl.CostEstimate(flops=2**20, bytes_accessed=13 * 2**20, transcendentals=0),
+    )(*(pltpu.with_memory_space_constraint(r, pltpu.VMEM) for r in results))
 
 
 def plain_body(

time: 195 us -> 184 us (0.944)
  local copies, waits for them, and re-layouts: 10.8 us -> 0 us
    unnamed x16 -> x0, local copies, waits for them, and re-layouts: 10.8 us -> none
    pallas_call x1 -> x2, Pallas kernels: 182 us -> 182 us  [the longest x1 177 us: fast_body(): pl.pallas_call(functools.partial(kernel, n_fs, n_tp), out_shape=(pltpu.VM...]
where the time goes in v1:
time: 184 us
  Pallas kernels  182 us (99%)
    pallas_call x1, Pallas kernels, fast_body(): pl.pallas_call(functools.partial(kernel, n_fs, n_tp), out_shape=(pltpu.VM...  177 us
    pallas_call x1, Pallas kernels, fast_body(): pl.pallas_call(store_kernel, out_shape=tuple((jax.ShapeDtypeStruct(r.shap...  4.61 us

profile of v1, /device:TPU:0, one launch (start us, length us, event | category | flops | bytes accessed | tf_op | source)
XLA Modules:
  0.0 184.0 jit_solution(10167325068936383641)
XLA Ops:
  0.6 1.6 pad_maximum_fusion.factor_ref
  2.2 177.2 %shard_map.145 = (f32[384,768]{1,0:T(8,128)S(1)}, f32[768,384]{1,0:T(8,128)S(1)}, bf16[3072,768]{1,0:T(8,128)(2,1)S(1)}, bf16[768,3072]{1,0:T(8,128)(2,1)S(1)}, ...) custom-call(bf16[512,3072]{1,0:T(8,128)(2,1)} %saved_hbm.1, bf16[512,3072]{1,0:T(8,128)(2,1)} %outcot_hbm.1, ...), custom_call_target="tpu_custom_call" | custom-call | flops 3019898880 | bytes 209715200 | tf_op jit(solution)/shard_map/pallas_call | solution.py:401
  179.4 4.6 %shard_map.146 = (f32[384,768]{1,0:T(8,128)}, f32[768,384]{1,0:T(8,128)}, bf16[3072,768]{1,0:T(8,128)(2,1)}, bf16[768,3072]{1,0:T(8,128)(2,1)}, f32[2,48,768]{2,1,0:T(8,128)}, /*index=5*/f32[2,48,768]{2,1,0:T(8,128)}) custom-call(f32[384,768]{1,0:T(8,128)S(1)} %get-tuple-element.12.refs_0_, f32[768,384]{1,0:T(8,128)S(1)} %get-tuple-element.13.refs_1_, ...), custom_call_target="tpu_custom_call" | custom-call | flops 1048576 | bytes 13631488 | tf_op jit(solution)/shard_map/pallas_call | solution.py:460

commit v2 on v1

--- a/solution.py
+++ b/solution.py
@@ -9,6 +9,10 @@
 
 MESH = pl.DeviceIdType.MESH
 PAIR = 2
+LINE = 4
+LANES = 128
+EARLY_QUERY = 1
+EARLY_OUT = 1
 NT = (((1,), (1,)), ((), ()))
 TN = (((0,), (0,)), ((), ()))
 
@@ -84,9 +88,113 @@
             self.inward(offset).wait_send()
 
 
+class Place:
+    def __init__(self, outer):
+        me, self.column = lax.axis_index("fs"), lax.axis_index("tp")
+        self.me, self.low, self.outer = me, lax.rem(me, PAIR), outer
+        self.z = me // PAIR
+        self.near = self.z + 1 - 2 * lax.rem(self.z, 2)
+        self.cross = outer - 1 - self.z
+        self.skew = outer - 1 - self.near
+        self.end = jnp.logical_or(self.z == 0, self.z == outer - 1)
+        self.inner = jnp.logical_not(self.end)
+
+    def same(self, z):
+        return z * PAIR + self.low
+
+    def other(self, z):
+        return z * PAIR + 1 - self.low
+
+
+class Spread:
+    def __init__(self, place, view, sends, recvs, odd, own=None):
+        self.place, self.view, self.sends, self.recvs, self.odd = place, view, sends, recvs, odd
+        self.own = view(place.me) if own is None else own
+
+    def copy(self, block, send, recv, target):
+        return pltpu.make_async_remote_copy(
+            src_ref=self.own if block is None else self.view(block),
+            dst_ref=self.view(self.place.me if block is None else block),
+            send_sem=self.sends.at[send],
+            recv_sem=self.recvs.at[recv],
+            device_id=(target, self.place.column),
+            device_id_type=MESH,
+        )
+
+    def to_skew(self):
+        return self.copy(None, 0, 0, self.place.same(self.place.skew))
+
+    def to_near(self):
+        return self.copy(None, 1, 1, self.place.same(self.place.near))
+
+    def to_cross(self):
+        return self.copy(None, 2, 2, self.place.same(self.place.cross))
+
+    def to_pair(self):
+        return self.copy(None, 3, 3, self.place.other(self.place.z))
+
+    def pair_skew(self):
+        return self.copy(self.place.same(self.place.skew), 4, 4, self.place.other(self.place.z))
+
+    def pair_near(self):
+        return self.copy(self.place.same(self.place.near), 5, 5, self.place.other(self.place.z))
+
+    def pair_cross(self):
+        return self.copy(self.place.same(self.place.cross), 6, 6, self.place.other(self.place.z))
+
+    def relay_skew(self):
+        return self.copy(self.place.same(self.place.skew), 7, 2, self.place.same(self.place.near))
+
+    def relay_pair(self):
+        return self.copy(self.place.other(self.place.z), 8, 5, self.place.same(self.place.near))
+
+    def when(self, condition, action):
+        if condition is True:
+            action()
+        elif condition is not False:
+            pl.when(condition)(action)
+
+    def launch(self):
+        self.to_pair().start()
+        self.to_skew().start()
+        self.to_near().start()
+        self.when(self.place.inner, lambda: self.to_cross().start())
+
+    def relay(self):
+        self.to_skew().wait_recv()
+        self.when(self.place.inner, lambda: self.relay_skew().start())
+        self.pair_skew().start()
+        self.to_near().wait_recv()
+        self.when(False if self.odd else self.place.end, lambda: self.pair_near().start())
+        self.to_pair().wait_recv()
+        self.when(True if self.odd else self.place.end, lambda: self.relay_pair().start())
+
+    def relay_last(self):
+        self.to_cross().wait_recv()
+        self.pair_cross().start()
+
+    def collect(self):
+        self.pair_skew().wait_recv()
+        self.pair_near().wait_recv()
+        self.pair_cross().wait_recv()
+
+    def drain(self):
+        self.to_pair().wait_send()
+        self.to_skew().wait_send()
+        self.to_near().wait_send()
+        self.pair_skew().wait_send()
+        self.pair_cross().wait_send()
+        self.when(self.place.inner, lambda: self.to_cross().wait_send())
+        self.when(self.place.inner, lambda: self.relay_skew().wait_send())
+        self.when(False if self.odd else self.place.end, lambda: self.pair_near().wait_send())
+        self.when(True if self.odd else self.place.end, lambda: self.relay_pair().wait_send())
+
+
 def kernel(
     n_fs,
     n_tp,
+    early_query,
+    early_out,
     saved_hbm,
     outcot_hbm,
     querycot_hbm,
@@ -103,6 +211,7 @@
     first_out,
     second_out,
     factors_ref,
+    own_rows,
     dirs_ref,
     query_master,
     out_master,
@@ -121,22 +230,24 @@
     own_dir,
     square_buf,
     load_sems,
-    factor_sems,
+    rows_sems,
     proj_sems,
     columns_sems,
     pair_sems,
     far_sems,
-    dir_sems,
     square_sems,
-    early_sems,
-    late_sems,
+    spread_sends,
+    spread_recvs,
 ):
-    me, column = lax.axis_index("fs"), lax.axis_index("tp")
-    high, low = me // PAIR, lax.rem(me, PAIR)
     outer = n_fs // PAIR
+    place = Place(outer)
+    me, column, high, low = place.me, place.column, place.z, place.low
     part = factor_ref.shape[1]
     width = factor_ref.shape[2]
     depth = first_ref.shape[1]
+    features = grad.shape[2]
+    pieces = width // LANES
+    tall, deep = LANES, features // pieces
     loads = [
         pltpu.make_async_copy(src, dst, load_sems.at[i])
         for i, (src, dst) in enumerate(
@@ -150,45 +261,73 @@
             )
         )
     ]
-    for load in loads[4:] + loads[:4]:
+    for load in loads:
         load.start()
 
-    peers = [(lax.rem(high + i, outer) * PAIR + low, column) for i in range(1, outer)]
-    peers.append((high * PAIR + 1 - low, column))
-    peers += [(me, lax.rem(column + i, n_tp)) for i in range(1, n_tp)]
+    fs_peers = [(lax.rem(me + i, n_fs), column) for i in range(1, n_fs)]
+    tp_peers = [(me, lax.rem(column + i, n_tp)) for i in range(1, n_tp)]
     barrier = pltpu.get_barrier_semaphore()
-    for peer in peers:
+    for peer in fs_peers + tp_peers:
         pl.semaphore_signal(barrier, inc=1, device_id=peer, device_id_type=MESH)
-    pl.semaphore_wait(barrier, len(peers))
-
-    factors = Gather(
-        "fs",
-        n_fs,
-        lambda i: factors_ref.at[:, rows(column, part), rows(i, width)],
-        factor_sems,
-        own=factor_ref,
-    )
-    factors.start()
+    pl.semaphore_wait(barrier, len(fs_peers) + len(tp_peers))
+
+    def spread(slot, view, odd, own=None):
+        return Spread(place, view, spread_sends.at[slot], spread_recvs.at[slot], odd, own)
+
+    factors = [
+        spread(
+            k,
+            lambda i, k=k: factors_ref.at[k, rows(column, part), rows(i, width)],
+            k == 1,
+            factor_ref.at[k],
+        )
+        for k in range(2)
+    ]
+    for gather in factors:
+        gather.launch()
+    own_columns = Gather("tp", n_tp, lambda i: own_rows.at[:, rows(i, part), :], rows_sems, own=factor_ref)
+    own_columns.start()
     factors_ref[:, rows(column, part), rows(me, width)] = factor_ref[...]
-
-    half = query_copy.shape[1] // 2
-    early = (
-        Gather("fs", n_fs, lambda i: query_copy.at[rows(i, width), :half], early_sems.at[0], own=query_early),
-        Gather("fs", n_fs, lambda i: out_copy.at[:half, rows(i, width)], early_sems.at[1], own=out_early),
-    )
+    own_rows[:, rows(column, part), :] = factor_ref[...]
+
+    def query_piece(i, own=None):
+        return spread(
+            4 + i,
+            lambda j: query_copy.at[pl.ds(pl.multiple_of(j * width + i * tall, tall), tall), :],
+            i % 2 == 1,
+            own,
+        )
+
+    def out_piece(i, own=None):
+        return spread(
+            4 + pieces + i,
+            lambda j: out_copy.at[i * deep : (i + 1) * deep, rows(j, width)],
+            (pieces + i) % 2 == 1,
+            own,
+        )
+
+    early_q = [query_piece(i, query_early.at[i]) for i in range(early_query)]
+    early_o = [out_piece(i, out_early.at[i]) for i in range(early_out)]
+    late_q = [query_piece(i) for i in range(early_query, pieces)]
+    late_o = [out_piece(i) for i in range(early_out, pieces)]
+
+    for gather in factors:
+        gather.relay()
     loads[4].wait()
-    query_early[...] = query_master[:, :half].astype(query_early.dtype)
+    for i in range(early_query):
+        query_early[i] = query_master[i * tall : (i + 1) * tall, :].astype(query_early.dtype)
     loads[5].wait()
-    out_early[...] = out_master[:half, :].astype(out_early.dtype)
-    for gather in early:
-        gather.start_outward()
-    factors.forward()
-    for gather in early:
-        gather.start_inward()
-    factors.finish()
+    for i in range(early_out):
+        out_early[i] = out_master[i * deep : (i + 1) * deep, :].astype(out_early.dtype)
+    for gather in factors:
+        gather.relay_last()
+    for gather in early_q:
+        gather.launch()
+    own_columns.forward()
 
     gathers = []
     for k, tokens in enumerate((saved, outcot)):
+        factors[k].collect()
         loads[k].wait()
         part_proj = lax.dot_general(
             factors_ref[k, rows(column, part), :],
@@ -202,162 +341,173 @@
         )
         gather.start()
         gathers.append(gather)
+
+    def pair_copy(offset, k):
+        return pltpu.make_async_remote_copy(
+            src_ref=pair_send.at[offset, k],
+            dst_ref=pair_recv.at[offset, k],
+            send_sem=pair_sems.at[0, offset, k],
+            recv_sem=pair_sems.at[1, offset, k],
+            device_id=(high * PAIR + 1 - low, column),
+            device_id_type=MESH,
+        )
+
+    def far_copy(offset, k):
+        return pltpu.make_async_remote_copy(
+            src_ref=far_send.at[offset, k],
+            dst_ref=far_recv.at[offset, k],
+            send_sem=far_sems.at[0, offset, k],
+            recv_sem=far_sems.at[1, offset, k],
+            device_id=(lax.rem(high + offset, outer) * PAIR + low, column),
+            device_id_type=MESH,
+        )
+
     columns = Gather("tp", n_tp, lambda i: factors_ref.at[:, rows(i, part), :], columns_sems)
-    for gather in gathers:
+    order = list(range(outer - 1, 0, -1)) + [0]
+    for k, (gather, cot) in enumerate(zip(gathers, (querycot, attn))):
         gather.forward()
-    columns.start()
-    for k, (gather, cot) in enumerate(zip(gathers, (querycot, attn))):
+        if k == 1:
+            columns.start()
         gather.finish()
         loads[2 + k].wait()
         grad[k, :, :] = jnp.dot(proj[k], cot[...], preferred_element_type=jnp.float32)
-
-    def pair_copy(offset):
-        return pltpu.make_async_remote_copy(
-            src_ref=pair_send.at[offset],
-            dst_ref=pair_recv.at[offset],
-            send_sem=pair_sems.at[0, offset],
-            recv_sem=pair_sems.at[1, offset],
-            device_id=(high * PAIR + 1 - low, column),
-            device_id_type=MESH,
-        )
-
-    def far_copy(offset):
-        return pltpu.make_async_remote_copy(
-            src_ref=far_send.at[offset],
-            dst_ref=far_recv.at[offset],
-            send_sem=far_sems.at[0, offset],
-            recv_sem=far_sems.at[1, offset],
-            device_id=(lax.rem(high + offset, outer) * PAIR + low, column),
-            device_id_type=MESH,
-        )
-
-    order = list(range(outer - 1, 0, -1)) + [0]
-    for offset in order:
-        target = lax.rem(high + offset, outer) * PAIR + 1 - low
-        pair_send[offset] = grad[:, rows(target, depth), :].astype(pair_send.dtype)
-        pair_copy(offset).start()
-    for offset in order:
-        target = lax.rem(high + offset, outer) * PAIR + low
-        pair_copy(offset).wait_recv()
-        both = grad[:, rows(target, depth), :] + pair_recv[offset].astype(jnp.float32)
-        if offset:
-            far_send[offset] = both.astype(far_send.dtype)
-            far_copy(offset).start()
-    total = both
-    columns.forward()
-    for gather in early:
-        gather.forward()
-    for offset in range(1, outer):
-        far_copy(offset).wait_recv()
-        total = total + far_recv[offset].astype(jnp.float32)
-
-    first_new, second_new, direction = moment_step(first_ref[...], second_ref[...], total)
-    own_dir[...] = direction.astype(own_dir.dtype)
-    spread = Gather("fs", n_fs, lambda i: dirs_ref.at[:, rows(i, depth), :], dir_sems, own=own_dir)
-    spread.start()
-    dirs_ref[:, rows(me, depth), :] = own_dir[...]
-    first_out[...] = first_new
-    second_out[...] = second_new
-    squares = direction * direction
+        for offset in order:
+            target = lax.rem(high + offset, outer) * PAIR + 1 - low
+            pair_send[offset, k] = grad[k, rows(target, depth), :].astype(pair_send.dtype)
+            pair_copy(offset, k).start()
+    totals = []
+    for k in range(2):
+        for offset in order:
+            target = lax.rem(high + offset, outer) * PAIR + low
+            pair_copy(offset, k).wait_recv()
+            both = grad[k, rows(target, depth), :] + pair_recv[offset, k].astype(jnp.float32)
+            if offset:
+                far_send[offset, k] = both.astype(far_send.dtype)
+                far_copy(offset, k).start()
+        totals.append(both)
+    for gather in early_q:
+        gather.relay()
+    for k in range(2):
+        for offset in range(1, outer):
+            far_copy(offset, k).wait_recv()
+            totals[k] = totals[k] + far_recv[offset, k].astype(jnp.float32)
+
     shape = square_buf.shape[1:]
     row = lax.broadcasted_iota(jnp.int32, shape, 0)
-    mine = jnp.where(row == 0, jnp.sum(squares[0]), jnp.sum(squares[1]))
-
-    rounds = (
-        [(me, lax.rem(column + i, n_tp)) for i in range(1, n_tp)],
-        [(lax.rem(high + i, outer) * PAIR + low, column) for i in range(1, outer)],
-        [(high * PAIR + 1 - low, column)],
-    )
-    slot = 0
-    tiny = []
-    for stage, targets in enumerate(rounds):
-        square_buf[slot] = mine
-        base = slot
-        copies = []
-        for target in targets:
-            slot += 1
-            copies.append(
-                pltpu.make_async_remote_copy(
-                    src_ref=square_buf.at[base],
-                    dst_ref=square_buf.at[slot],
-                    send_sem=square_sems.at[0, slot],
-                    recv_sem=square_sems.at[1, slot],
-                    device_id=target,
-                    device_id_type=MESH,
-                )
+    mine = jnp.zeros(shape, jnp.float32)
+    for k in range(2):
+        first_new, second_new, direction = moment_step(first_ref[k], second_ref[k], totals[k])
+        own_dir[k] = direction.astype(own_dir.dtype)
+        first_out[k] = first_new
+        second_out[k] = second_new
+        mine = jnp.where(row == k, jnp.sum(direction * direction), mine)
+
+    def square_copies(base, targets):
+        return [
+            pltpu.make_async_remote_copy(
+                src_ref=square_buf.at[base],
+                dst_ref=square_buf.at[base + 1 + i],
+                send_sem=square_sems.at[0, base + 1 + i],
+                recv_sem=square_sems.at[1, base + 1 + i],
+                device_id=target,
+                device_id_type=MESH,
             )
-        for copy in copies:
-            copy.start()
-        if stage == 1:
-            spread.forward()
-        for i, copy in enumerate(copies):
-            copy.wait_recv()
-            mine = mine + square_buf[base + 1 + i]
-        tiny += copies
-        slot += 1
-    spread.finish()
-    columns.finish()
-
+            for i, target in enumerate(targets)
+        ]
+
+    square_buf[0] = mine
+    square_fs = square_copies(0, fs_peers)
+    for copy in square_fs:
+        copy.start()
+    dirs = [
+        spread(2 + k, lambda i, k=k: dirs_ref.at[k, rows(i, depth), :], k == 1, own_dir.at[k]) for k in range(2)
+    ]
+    for gather in dirs:
+        gather.launch()
+    dirs_ref[:, rows(me, depth), :] = own_dir[...]
+    for i, copy in enumerate(square_fs):
+        copy.wait_recv()
+        mine = mine + square_buf[1 + i]
+    square_buf[n_fs] = mine
+    square_tp = square_copies(n_fs, tp_peers)
+    for copy in square_tp:
+        copy.start()
+    for gather in dirs:
+        gather.relay()
+    for gather in early_q:
+        gather.relay_last()
+    for gather in dirs:
+        gather.relay_last()
+    for gather in early_o:
+        gather.launch()
+    for i, copy in enumerate(square_tp):
+        copy.wait_recv()
+        mine = mine + square_buf[n_fs + 1 + i]
     entries = dirs_ref.shape[1] * dirs_ref.shape[2] * n_tp
     scale = 0.01 * lax.rsqrt(mine / entries + 1e-06)
-    query_scale, out_scale = scale[0:1, 0:1], scale[1:2, 0:1]
-
-    def step(k, block, part_of_features):
-        factor = factors_ref[k, :, rows(block, width)]
-        direction = dirs_ref[k, :, part_of_features]
-        pair = (factor, direction) if k == 0 else (direction, factor)
-        return lax.dot_general(*pair, TN, preferred_element_type=jnp.float32)
-
-    tall, deep = width // 2, half // 2
-    late_query = [
-        Gather("fs", n_fs, lambda i, p=p: query_copy.at[rows(2 * i + p, tall), half:], late_sems.at[p])
-        for p in range(2)
-    ]
-    late_out = [
-        Gather(
-            "fs",
-            n_fs,
-            lambda i, p=p: out_copy.at[half + p * deep : half + (p + 1) * deep, rows(i, width)],
-            late_sems.at[2 + p],
-        )
-        for p in range(2)
-    ]
-    late = late_query + late_out
-    for part_of_features in (slice(half, None), slice(0, half)):
-        query_new = query_master[:, part_of_features] - query_scale * step(0, me, part_of_features)
-        query_out[:, part_of_features] = query_new
-        query_copy[rows(me, width), part_of_features] = query_new.astype(query_copy.dtype)
-        if part_of_features.start:
-            for gather in late_query:
-                gather.start()
-        out_new = out_master[part_of_features, :] - out_scale * step(1, me, part_of_features)
-        out_out[part_of_features, :] = out_new
-        out_copy[part_of_features, rows(me, width)] = out_new.astype(out_copy.dtype)
-        if part_of_features.start:
-            for gather in late_out:
-                gather.start()
-    for gather in early:
-        gather.finish()
+    scales = (scale[0:1, 0:1], scale[1:2, 0:1])
+    own_columns.finish()
+    for gather in dirs:
+        gather.collect()
+
+    query_new = query_master[...] - scales[0] * lax.dot_general(
+        own_rows[0], dirs_ref[0], TN, preferred_element_type=jnp.float32
+    )
+    query_out[...] = query_new
+    query_copy[rows(me, width), :] = query_new.astype(query_copy.dtype)
+    for gather in late_q:
+        gather.launch()
+    out_new = out_master[...] - scales[1] * lax.dot_general(
+        dirs_ref[1], own_rows[1], TN, preferred_element_type=jnp.float32
+    )
+    out_out[...] = out_new
+    out_copy[:, rows(me, width)] = out_new.astype(out_copy.dtype)
+    for gather in late_o:
+        gather.launch()
+
+    columns.forward()
+    for gather in early_o + late_q + late_o:
+        gather.relay()
+    for gather in early_o + late_q + late_o:
+        gather.relay_last()
+    columns.finish()
+
+    for gather in early_q + early_o:
+        gather.collect()
+        gather.drain()
 
     def finish_block(i, carry):
         block = lax.rem(me + i, n_fs)
-        where = rows(block, width)
-        query = query_copy[where, :half].astype(jnp.float32)
-        query_copy[where, :half] = (query - query_scale * step(0, block, slice(0, half))).astype(query_copy.dtype)
-        out = out_copy[:half, where].astype(jnp.float32)
-        out_copy[:half, where] = (out - out_scale * step(1, block, slice(0, half))).astype(out_copy.dtype)
+        for j in range(early_query):
+            where = pl.ds(pl.multiple_of(block * width + j * tall, tall), tall)
+            step = lax.dot_general(
+                factors_ref[0, :, where], dirs_ref[0], TN, preferred_element_type=jnp.float32
+            )
+            query = query_copy[where, :].astype(jnp.float32)
+            query_copy[where, :] = (query - scales[0] * step).astype(query_copy.dtype)
+        for j in range(early_out):
+            band = slice(j * deep, (j + 1) * deep)
+            step = lax.dot_general(
+                dirs_ref[1, :, band],
+                factors_ref[1, :, rows(block, width)],
+                TN,
+                preferred_element_type=jnp.float32,
+            )
+            out = out_copy[band, rows(block, width)].astype(jnp.float32)
+            out_copy[band, rows(block, width)] = (out - scales[1] * step).astype(out_copy.dtype)
         return carry
 
     lax.fori_loop(1, n_fs, finish_block, 0)
-    for gather in late:
-        gather.forward()
-    for gather in late:
-        gather.finish()
-    for offset in order:
-        pair_copy(offset).wait_send()
-        if offset:
-            far_copy(offset).wait_send()
-    for copy in tiny:
+    for gather in late_q + late_o:
+        gather.collect()
+    for gather in factors + dirs + late_q + late_o:
+        gather.drain()
+    for k in range(2):
+        for offset in order:
+            pair_copy(offset, k).wait_send()
+            if offset:
+                far_copy(offset, k).wait_send()
+    for copy in square_fs + square_tp:
         copy.wait_send()
 
 
@@ -391,15 +541,14 @@
     depth = first_moment.shape[1]
     rank = part * n_tp
     outer = n_fs // PAIR
-    half = features // 2
+    pieces = width // LANES
     low, wide = jnp.bfloat16, jnp.float32
     vmem = pl.BlockSpec(memory_space=pltpu.VMEM)
     anywhere = pl.BlockSpec(memory_space=pl.ANY)
     dma = pltpu.SemaphoreType.DMA
-    tiny_slots = n_tp + outer + PAIR
     factor = jnp.stack([left_factor.T, right_factor.T])
     results = pl.pallas_call(
-        functools.partial(kernel, n_fs, n_tp),
+        functools.partial(kernel, n_fs, n_tp, EARLY_QUERY, EARLY_OUT),
         out_shape=(
             pltpu.VMEM((width, features), wide),
             pltpu.VMEM((features, width), wide),
@@ -412,11 +561,12 @@
         out_specs=(vmem,) * 6,
         scratch_shapes=[
             pltpu.VMEM((2, rank, model), low),
+            pltpu.VMEM((2, rank, width), low),
             pltpu.VMEM((2, rank, features), low),
             pltpu.VMEM((width, features), wide),
             pltpu.VMEM((features, width), wide),
-            pltpu.VMEM((width, half), low),
-            pltpu.VMEM((half, width), low),
+            pltpu.VMEM((max(EARLY_QUERY, 1), LANES, features), low),
+            pltpu.VMEM((max(EARLY_OUT, 1), features // pieces, width), low),
             pltpu.VMEM((tokens, model), low),
             pltpu.VMEM((tokens, model), low),
             pltpu.VMEM((tokens, features), low),
@@ -428,17 +578,16 @@
             pltpu.VMEM((outer, 2, depth, features), low),
             pltpu.VMEM((outer, 2, depth, features), low),
             pltpu.VMEM((2, depth, features), low),
-            pltpu.VMEM((tiny_slots, 8, 128), wide),
+            pltpu.VMEM((n_fs + n_tp, 8, 128), wide),
             dma((6,)),
-            dma((2, 2, outer)),
+            dma((2, 2, n_tp // PAIR)),
             dma((2, 2, 2, n_tp // PAIR)),
             dma((2, 2, n_tp // PAIR)),
-            dma((2, outer)),
-            dma((2, outer)),
-            dma((2, 2, outer)),
-            dma((2, tiny_slots)),
-            dma((2, 2, 2, outer)),
-            dma((4, 2, 2, outer)),
+            dma((2, outer, 2)),
+            dma((2, outer, 2)),
+            dma((2, n_fs + n_tp)),
+            dma((4 + 2 * pieces, 9)),
+            dma((4 + 2 * pieces, 7)),
         ],
         compiler_params=pltpu.CompilerParams(
             collective_id=0, has_side_effects=True, vmem_limit_bytes=46 * 2**20
@@ -527,8 +676,8 @@
     model, part = args[0].shape[1], left_factor.shape[1]
     aligned = part % 16 == 0 and first_moment.shape[1] % 16 == 0
     aligned = aligned and model // n_fs % 128 == 0 and first_moment.shape[2] % 256 == 0
-    aligned = aligned and model // n_fs % 32 == 0 and first_moment.shape[2] % 64 == 0
-    if aligned and n_fs % PAIR == 0 and n_tp % PAIR == 0:
+    aligned = aligned and first_moment.shape[2] % (model // n_fs) == 0
+    if aligned and n_fs == PAIR * LINE and n_tp % PAIR == 0:
         return fast_body(n_fs, n_tp, *args)
     return plain_body(*args)
 

time: 184 us -> 154 us (0.84)
  Pallas kernels: 182 us -> 152 us
    pallas_call x1, Pallas kernels: 177 us -> 147 us  [fast_body(): pl.pallas_call(functools.partial(kernel, n_fs, n_tp, EARLY_QUERY, EARLY_O...]
where the time goes in v2:
time: 154 us
  Pallas kernels  152 us (99%)
  other arithmetic  1.6 us (1%)
    pallas_call x1, Pallas kernels, fast_body(): pl.pallas_call(functools.partial(kernel, n_fs, n_tp, EARLY_QUERY, EARLY_O...  147 us
    pallas_call x1, Pallas kernels, fast_body(): pl.pallas_call(store_kernel, out_shape=tuple((jax.ShapeDtypeStruct(r.shap...  4.61 us

profile of v2, /device:TPU:0, one launch (start us, length us, event | category | flops | bytes accessed | tf_op | source)
XLA Modules:
  0.0 153.9 jit_solution(15890854635488412531)
XLA Ops:
  0.6 1.6 %pad_maximum_fusion.factor_ref = bf16[2,96,384]{2,1,0:T(8,128)(2,1)} fusion(bf16[1,96,384]{2,1,0:T(8,128)(2,1)} %bitcast.6, bf16[1,96,384]{2,1,0:T(8,128)(2,1)} %bitcast.7), kind=kLoop, calls=%fused_computation | loop fusion | flops 73728 | bytes 294912 | tf_op jit(solution)/shard_map/stack | solution.py:549
  2.2 147.0 %shard_map.145 = (f32[384,768]{1,0:T(8,128)S(1)}, f32[768,384]{1,0:T(8,128)S(1)}, bf16[3072,768]{1,0:T(8,128)(2,1)S(1)}, bf16[768,3072]{1,0:T(8,128)(2,1)S(1)}, ...) custom-call(bf16[512,3072]{1,0:T(8,128)(2,1)} %saved_hbm.1, bf16[512,3072]{1,0:T(8,128)(2,1)} %outcot_hbm.1, ...), custom_call_target="tpu_custom_call" | custom-call | flops 3019898880 | bytes 209715200 | tf_op jit(solution)/shard_map/pallas_call | solution.py:550
  149.3 4.6 %shard_map.146 = (f32[384,768]{1,0:T(8,128)}, f32[768,384]{1,0:T(8,128)}, bf16[3072,768]{1,0:T(8,128)(2,1)}, bf16[768,3072]{1,0:T(8,128)(2,1)}, f32[2,48,768]{2,1,0:T(8,128)}, /*index=5*/f32[2,48,768]{2,1,0:T(8,128)}) custom-call(f32[384,768]{1,0:T(8,128)S(1)} %get-tuple-element.12.refs_0_, f32[768,384]{1,0:T(8,128)S(1)} %get-tuple-element.13.refs_1_, ...), custom_call_target="tpu_custom_call" | custom-call | flops 1048576 | bytes 13631488 | tf_op jit(solution)/shard_map/pallas_call | solution.py:609

commit v3 on v2

--- a/solution.py
+++ b/solution.py
@@ -13,6 +13,9 @@
 LANES = 128
 EARLY_QUERY = 1
 EARLY_OUT = 1
+STORES = 4
+QUERY_ODD = (True,False,True)
+OUT_ODD = (True,False,True)
 NT = (((1,), (1,)), ((), ()))
 TN = (((0,), (0,)), ((), ()))
 
@@ -107,87 +110,108 @@
 
 
 class Spread:
-    def __init__(self, place, view, sends, recvs, odd, own=None):
-        self.place, self.view, self.sends, self.recvs, self.odd = place, view, sends, recvs, odd
+    def __init__(self, place, view, span, send_sem, recv_sems, odd, own=None):
+        self.place, self.view, self.span, self.odd = place, view, span, odd
+        self.send_sem, self.recv_sems = send_sem, recv_sems
         self.own = view(place.me) if own is None else own
 
-    def copy(self, block, send, recv, target):
+    def remote(self, src, dst, recv, target):
         return pltpu.make_async_remote_copy(
-            src_ref=self.own if block is None else self.view(block),
-            dst_ref=self.view(self.place.me if block is None else block),
-            send_sem=self.sends.at[send],
-            recv_sem=self.recvs.at[recv],
+            src_ref=src,
+            dst_ref=dst,
+            send_sem=self.send_sem,
+            recv_sem=self.recv_sems.at[recv],
             device_id=(target, self.place.column),
             device_id_type=MESH,
         )
 
+    def mine(self, recv, target):
+        return self.remote(self.own, self.view(self.place.me), recv, target)
+
+    def passed(self, block, recv, target):
+        return self.remote(self.view(block), self.view(block), recv, target)
+
     def to_skew(self):
-        return self.copy(None, 0, 0, self.place.same(self.place.skew))
+        return self.mine(0, self.place.same(self.place.skew))
 
     def to_near(self):
-        return self.copy(None, 1, 1, self.place.same(self.place.near))
+        return self.mine(1, self.place.same(self.place.near))
 
     def to_cross(self):
-        return self.copy(None, 2, 2, self.place.same(self.place.cross))
+        return self.mine(2, self.place.same(self.place.cross))
 
     def to_pair(self):
-        return self.copy(None, 3, 3, self.place.other(self.place.z))
-
-    def pair_skew(self):
-        return self.copy(self.place.same(self.place.skew), 4, 4, self.place.other(self.place.z))
-
-    def pair_near(self):
-        return self.copy(self.place.same(self.place.near), 5, 5, self.place.other(self.place.z))
-
-    def pair_cross(self):
-        return self.copy(self.place.same(self.place.cross), 6, 6, self.place.other(self.place.z))
+        return self.mine(3, self.place.other(self.place.z))
+
+    def pair_on(self, z):
+        return self.passed(self.place.same(z), 4, self.place.other(self.place.z))
 
     def relay_skew(self):
-        return self.copy(self.place.same(self.place.skew), 7, 2, self.place.same(self.place.near))
+        return self.passed(self.place.same(self.place.skew), 2, self.place.same(self.place.near))
 
     def relay_pair(self):
-        return self.copy(self.place.other(self.place.z), 8, 5, self.place.same(self.place.near))
-
-    def when(self, condition, action):
-        if condition is True:
-            action()
-        elif condition is not False:
-            pl.when(condition)(action)
+        return self.passed(self.place.other(self.place.z), 4, self.place.same(self.place.near))
 
     def launch(self):
+        self.launch_pair()
+        self.launch_skew()
+        self.launch_near()
+        self.launch_cross()
+
+    def launch_pair(self):
         self.to_pair().start()
+
+    def launch_skew(self):
         self.to_skew().start()
+
+    def launch_near(self):
         self.to_near().start()
-        self.when(self.place.inner, lambda: self.to_cross().start())
+
+    def launch_cross(self):
+        pl.when(self.place.inner)(lambda: self.to_cross().start())
+
+    def hop(self):
+        self.to_skew().wait_recv()
+        pl.when(self.place.inner)(lambda: self.relay_skew().start())
+
+    def pass_skew(self):
+        self.pair_on(self.place.skew).start()
+
+    def pass_near(self):
+        if not self.odd:
+            self.to_near().wait_recv()
+            pl.when(self.place.end)(lambda: self.pair_on(self.place.near).start())
+
+    def pass_pair(self):
+        self.to_pair().wait_recv()
+        if self.odd:
+            self.relay_pair().start()
+        else:
+            pl.when(self.place.end)(lambda: self.relay_pair().start())
+
+    def pass_cross(self):
+        self.to_cross().wait_recv()
+        self.pair_on(self.place.cross).start()
 
     def relay(self):
-        self.to_skew().wait_recv()
-        self.when(self.place.inner, lambda: self.relay_skew().start())
-        self.pair_skew().start()
-        self.to_near().wait_recv()
-        self.when(False if self.odd else self.place.end, lambda: self.pair_near().start())
-        self.to_pair().wait_recv()
-        self.when(True if self.odd else self.place.end, lambda: self.relay_pair().start())
-
-    def relay_last(self):
-        self.to_cross().wait_recv()
-        self.pair_cross().start()
+        self.hop()
+        self.pass_skew()
+        self.pass_near()
+
+    def many(self, count):
+        return self.remote(self.span(count), self.span(count), 4, self.place.other(self.place.z))
 
     def collect(self):
-        self.pair_skew().wait_recv()
-        self.pair_near().wait_recv()
-        self.pair_cross().wait_recv()
+        if self.odd:
+            self.to_near().wait_recv()
+        self.many(3).wait_recv()
 
     def drain(self):
-        self.to_pair().wait_send()
-        self.to_skew().wait_send()
-        self.to_near().wait_send()
-        self.pair_skew().wait_send()
-        self.pair_cross().wait_send()
-        self.when(self.place.inner, lambda: self.to_cross().wait_send())
-        self.when(self.place.inner, lambda: self.relay_skew().wait_send())
-        self.when(False if self.odd else self.place.end, lambda: self.pair_near().wait_send())
-        self.when(True if self.odd else self.place.end, lambda: self.relay_pair().wait_send())
+        if self.odd:
+            pl.when(self.place.end)(lambda: self.many(6).wait_send())
+            pl.when(self.place.inner)(lambda: self.many(8).wait_send())
+        else:
+            self.many(7).wait_send()
 
 
 def kernel(
@@ -201,15 +225,19 @@
     attn_hbm,
     query_hbm,
     out_hbm,
-    factor_ref,
-    first_ref,
-    second_ref,
+    left_hbm,
+    right_hbm,
+    first_hbm,
+    second_hbm,
     query_out,
     out_out,
     query_copy,
     out_copy,
     first_out,
     second_out,
+    factor_ref,
+    first_ref,
+    second_ref,
     factors_ref,
     own_rows,
     dirs_ref,
@@ -235,6 +263,7 @@
     columns_sems,
     pair_sems,
     far_sems,
+    wire_sems,
     square_sems,
     spread_sends,
     spread_recvs,
@@ -258,10 +287,14 @@
                 (attn_hbm, attn),
                 (query_hbm, query_master),
                 (out_hbm, out_master),
+                (first_hbm, first_ref),
+                (second_hbm, second_ref),
+                (left_hbm, factor_ref.at[0]),
+                (right_hbm, factor_ref.at[1]),
             )
         )
     ]
-    for load in loads:
+    for load in loads[8:] + loads[:8]:
         load.start()
 
     fs_peers = [(lax.rem(me + i, n_fs), column) for i in range(1, n_fs)]
@@ -269,15 +302,18 @@
     barrier = pltpu.get_barrier_semaphore()
     for peer in fs_peers + tp_peers:
         pl.semaphore_signal(barrier, inc=1, device_id=peer, device_id_type=MESH)
+    for load in loads[8:]:
+        load.wait()
     pl.semaphore_wait(barrier, len(fs_peers) + len(tp_peers))
 
-    def spread(slot, view, odd, own=None):
-        return Spread(place, view, spread_sends.at[slot], spread_recvs.at[slot], odd, own)
+    def spread(slot, view, span, odd, own=None):
+        return Spread(place, view, span, spread_sends.at[slot], spread_recvs.at[slot], odd, own)
 
     factors = [
         spread(
             k,
             lambda i, k=k: factors_ref.at[k, rows(column, part), rows(i, width)],
+            lambda n, k=k: factors_ref.at[k, :part, : n * width],
             k == 1,
             factor_ref.at[k],
         )
@@ -294,7 +330,8 @@
         return spread(
             4 + i,
             lambda j: query_copy.at[pl.ds(pl.multiple_of(j * width + i * tall, tall), tall), :],
-            i % 2 == 1,
+            lambda n: query_copy.at[: n * tall, :],
+            QUERY_ODD[i % 3],
             own,
         )
 
@@ -302,7 +339,8 @@
         return spread(
             4 + pieces + i,
             lambda j: out_copy.at[i * deep : (i + 1) * deep, rows(j, width)],
-            (pieces + i) % 2 == 1,
+            lambda n: out_copy.at[:deep, : n * width],
+            OUT_ODD[i % 3],
             own,
         )
 
@@ -311,18 +349,24 @@
     late_q = [query_piece(i) for i in range(early_query, pieces)]
     late_o = [out_piece(i) for i in range(early_out, pieces)]
 
-    for gather in factors:
-        gather.relay()
     loads[4].wait()
     for i in range(early_query):
         query_early[i] = query_master[i * tall : (i + 1) * tall, :].astype(query_early.dtype)
     loads[5].wait()
     for i in range(early_out):
         out_early[i] = out_master[i * deep : (i + 1) * deep, :].astype(out_early.dtype)
+    for gather in early_q:
+        gather.launch_pair()
     for gather in factors:
-        gather.relay_last()
+        gather.relay()
+    for gather in factors:
+        gather.pass_pair()
+    for gather in factors:
+        gather.pass_cross()
     for gather in early_q:
-        gather.launch()
+        gather.launch_skew()
+        gather.launch_near()
+        gather.launch_cross()
     own_columns.forward()
 
     gathers = []
@@ -342,28 +386,32 @@
         gather.start()
         gathers.append(gather)
 
-    def pair_copy(offset, k):
+    blocks = (place.cross, place.skew, place.near, place.z)
+
+    def pair_copy(r, k):
         return pltpu.make_async_remote_copy(
-            src_ref=pair_send.at[offset, k],
-            dst_ref=pair_recv.at[offset, k],
-            send_sem=pair_sems.at[0, offset, k],
-            recv_sem=pair_sems.at[1, offset, k],
-            device_id=(high * PAIR + 1 - low, column),
+            src_ref=pair_send.at[r, k],
+            dst_ref=pair_recv.at[r, k],
+            send_sem=wire_sems.at[0],
+            recv_sem=pair_sems.at[r, k],
+            device_id=(place.other(place.z), column),
             device_id_type=MESH,
         )
 
-    def far_copy(offset, k):
+    def far_copy(r, k, slot, z):
         return pltpu.make_async_remote_copy(
-            src_ref=far_send.at[offset, k],
-            dst_ref=far_recv.at[offset, k],
-            send_sem=far_sems.at[0, offset, k],
-            recv_sem=far_sems.at[1, offset, k],
-            device_id=(lax.rem(high + offset, outer) * PAIR + low, column),
+            src_ref=far_send.at[r, k],
+            dst_ref=far_recv.at[slot, k],
+            send_sem=wire_sems.at[1],
+            recv_sem=far_sems.at[slot, k],
+            device_id=(place.same(z), column),
             device_id_type=MESH,
         )
 
+    def both(r, k):
+        return grad[k, rows(place.same(blocks[r]), depth), :] + pair_recv[r, k].astype(jnp.float32)
+
     columns = Gather("tp", n_tp, lambda i: factors_ref.at[:, rows(i, part), :], columns_sems)
-    order = list(range(outer - 1, 0, -1)) + [0]
     for k, (gather, cot) in enumerate(zip(gathers, (querycot, attn))):
         gather.forward()
         if k == 1:
@@ -371,30 +419,43 @@
         gather.finish()
         loads[2 + k].wait()
         grad[k, :, :] = jnp.dot(proj[k], cot[...], preferred_element_type=jnp.float32)
-        for offset in order:
-            target = lax.rem(high + offset, outer) * PAIR + 1 - low
-            pair_send[offset, k] = grad[k, rows(target, depth), :].astype(pair_send.dtype)
-            pair_copy(offset, k).start()
+        for r in range(outer):
+            pair_send[r, k] = grad[k, rows(place.other(blocks[r]), depth), :].astype(pair_send.dtype)
+            pair_copy(r, k).start()
     totals = []
     for k in range(2):
-        for offset in order:
-            target = lax.rem(high + offset, outer) * PAIR + low
-            pair_copy(offset, k).wait_recv()
-            both = grad[k, rows(target, depth), :] + pair_recv[offset, k].astype(jnp.float32)
-            if offset:
-                far_send[offset, k] = both.astype(far_send.dtype)
-                far_copy(offset, k).start()
-        totals.append(both)
+        for r in range(outer - 1):
+            pair_copy(r, k).wait_recv()
+            far_send[r, k] = both(r, k).astype(far_send.dtype)
+            if r == outer - 2:
+                far_copy(r, k, 2, place.near).start()
+            else:
+                pl.when(place.end)(lambda r=r, k=k: far_copy(r, k, 1 - r, place.near).start())
+        pair_copy(outer - 1, k).wait_recv()
+        totals.append(both(outer - 1, k))
+
+        def add_near(k=k):
+            for r in range(outer - 2):
+                far_copy(r, k, r, place.near).wait_recv()
+                far_send[r, k] = (both(r, k) + far_recv[r, k].astype(jnp.float32)).astype(far_send.dtype)
+                far_copy(r, k, 3, blocks[r]).start()
+
+        pl.when(place.inner)(add_near)
+        if k == 0:
+            for gather in early_q:
+                gather.hop()
     for gather in early_q:
-        gather.relay()
+        gather.pass_skew()
     for k in range(2):
-        for offset in range(1, outer):
-            far_copy(offset, k).wait_recv()
-            totals[k] = totals[k] + far_recv[offset, k].astype(jnp.float32)
+        for slot in (2, 3):
+            far_copy(0, k, slot, place.near).wait_recv()
+            totals[k] = totals[k] + far_recv[slot, k].astype(jnp.float32)
 
     shape = square_buf.shape[1:]
     row = lax.broadcasted_iota(jnp.int32, shape, 0)
     mine = jnp.zeros(shape, jnp.float32)
+    for load in loads[6:8]:
+        load.wait()
     for k in range(2):
         first_new, second_new, direction = moment_step(first_ref[k], second_ref[k], totals[k])
         own_dir[k] = direction.astype(own_dir.dtype)
@@ -402,47 +463,56 @@
         second_out[k] = second_new
         mine = jnp.where(row == k, jnp.sum(direction * direction), mine)
 
-    def square_copies(base, targets):
-        return [
-            pltpu.make_async_remote_copy(
-                src_ref=square_buf.at[base],
-                dst_ref=square_buf.at[base + 1 + i],
-                send_sem=square_sems.at[0, base + 1 + i],
-                recv_sem=square_sems.at[1, base + 1 + i],
-                device_id=target,
-                device_id_type=MESH,
-            )
-            for i, target in enumerate(targets)
-        ]
+    def square_copy(base, slot, stage, count, target):
+        return pltpu.make_async_remote_copy(
+            src_ref=square_buf.at[pl.ds(base, count)],
+            dst_ref=square_buf.at[pl.ds(slot, count)],
+            send_sem=square_sems.at[stage, 0],
+            recv_sem=square_sems.at[stage, 1],
+            device_id=target,
+            device_id_type=MESH,
+        )
+
+    def square_all(base, count, stage):
+        return square_copy(base, base + 1, stage, count, tp_peers[0])
 
     square_buf[0] = mine
-    square_fs = square_copies(0, fs_peers)
-    for copy in square_fs:
-        copy.start()
+    for i, peer in enumerate(fs_peers):
+        square_copy(0, 1 + i, 0, 1, peer).start()
     dirs = [
-        spread(2 + k, lambda i, k=k: dirs_ref.at[k, rows(i, depth), :], k == 1, own_dir.at[k]) for k in range(2)
+        spread(
+            2 + k,
+            lambda i, k=k: dirs_ref.at[k, rows(i, depth), :],
+            lambda n, k=k: dirs_ref.at[k, : n * depth, :],
+            k == 1,
+            own_dir.at[k],
+        )
+        for k in range(2)
     ]
     for gather in dirs:
         gather.launch()
     dirs_ref[:, rows(me, depth), :] = own_dir[...]
-    for i, copy in enumerate(square_fs):
-        copy.wait_recv()
-        mine = mine + square_buf[1 + i]
+    square_all(0, n_fs - 1, 0).wait_recv()
+    mine = jnp.sum(square_buf[:n_fs], axis=0)
     square_buf[n_fs] = mine
-    square_tp = square_copies(n_fs, tp_peers)
-    for copy in square_tp:
-        copy.start()
+    for i, peer in enumerate(tp_peers):
+        square_copy(n_fs, n_fs + 1 + i, 1, 1, peer).start()
     for gather in dirs:
         gather.relay()
+    for gather in dirs:
+        gather.pass_pair()
     for gather in early_q:
-        gather.relay_last()
+        gather.pass_near()
+        gather.pass_pair()
+    for gather in early_o:
+        gather.launch_skew()
+        gather.launch_cross()
     for gather in dirs:
-        gather.relay_last()
+        gather.pass_cross()
     for gather in early_o:
-        gather.launch()
-    for i, copy in enumerate(square_tp):
-        copy.wait_recv()
-        mine = mine + square_buf[n_fs + 1 + i]
+        gather.launch_pair()
+    square_all(n_fs, n_tp - 1, 1).wait_recv()
+    mine = jnp.sum(square_buf[n_fs:], axis=0)
     entries = dirs_ref.shape[1] * dirs_ref.shape[2] * n_tp
     scale = 0.01 * lax.rsqrt(mine / entries + 1e-06)
     scales = (scale[0:1, 0:1], scale[1:2, 0:1])
@@ -450,26 +520,49 @@
     for gather in dirs:
         gather.collect()
 
+    def launch_late(gathers):
+        for gather in gathers:
+            gather.launch_pair()
+            gather.launch_skew()
+            if not gather.odd:
+                gather.launch_near()
+
     query_new = query_master[...] - scales[0] * lax.dot_general(
         own_rows[0], dirs_ref[0], TN, preferred_element_type=jnp.float32
     )
     query_out[...] = query_new
     query_copy[rows(me, width), :] = query_new.astype(query_copy.dtype)
-    for gather in late_q:
-        gather.launch()
+    launch_late(late_q)
     out_new = out_master[...] - scales[1] * lax.dot_general(
         dirs_ref[1], own_rows[1], TN, preferred_element_type=jnp.float32
     )
     out_out[...] = out_new
     out_copy[:, rows(me, width)] = out_new.astype(out_copy.dtype)
-    for gather in late_o:
-        gather.launch()
+    launch_late(late_o)
+    for gather in late_q + late_o:
+        gather.launch_cross()
 
     columns.forward()
-    for gather in early_o + late_q + late_o:
+    bulk = early_o + late_q + late_o
+
+    def finish_near(gather):
+        if gather.odd:
+            gather.launch_near()
+        gather.pass_pair()
+
+    crossing = early_q + bulk
+    for i, gather in enumerate(bulk):
         gather.relay()
-    for gather in early_o + late_q + late_o:
-        gather.relay_last()
+        if i >= 1:
+            pl.when(place.end)(crossing[i + 1 - 2].pass_cross)
+        if i >= 3:
+            finish_near(bulk[i - 3])
+    for gather in bulk[max(len(bulk) - 3, 0) :]:
+        finish_near(gather)
+    for gather in crossing[:-2]:
+        pl.when(place.inner)(gather.pass_cross)
+    for gather in crossing[-2:]:
+        gather.pass_cross()
     columns.finish()
 
     for gather in early_q + early_o:
@@ -502,19 +595,21 @@
         gather.collect()
     for gather in factors + dirs + late_q + late_o:
         gather.drain()
-    for k in range(2):
-        for offset in order:
-            pair_copy(offset, k).wait_send()
-            if offset:
-                far_copy(offset, k).wait_send()
-    for copy in square_fs + square_tp:
-        copy.wait_send()
+    pltpu.make_async_copy(pair_send, pair_recv, wire_sems.at[0]).wait()
+    pltpu.make_async_copy(far_send.at[1:], far_send.at[1:], wire_sems.at[1]).wait()
+    square_all(0, n_fs - 1, 0).wait_send()
+    square_all(n_fs, n_tp - 1, 1).wait_send()
 
 
 def store_kernel(*refs):
     count = len(refs) // 2
     sems = refs[-1]
-    copies = [pltpu.make_async_copy(refs[i], refs[count + i], sems.at[i]) for i in range(count)]
+    copies = []
+    for i in range(count):
+        size = refs[i].shape[0] // STORES if refs[i].shape[0] % (16 * STORES) == 0 else refs[i].shape[0]
+        for j in range(refs[i].shape[0] // size):
+            band = slice(j * size, (j + 1) * size)
+            copies.append(pltpu.make_async_copy(refs[i].at[band], refs[count + i].at[band], sems.at[i, j]))
     for copy in copies:
         copy.start()
     for copy in copies:
@@ -546,7 +641,6 @@
     vmem = pl.BlockSpec(memory_space=pltpu.VMEM)
     anywhere = pl.BlockSpec(memory_space=pl.ANY)
     dma = pltpu.SemaphoreType.DMA
-    factor = jnp.stack([left_factor.T, right_factor.T])
     results = pl.pallas_call(
         functools.partial(kernel, n_fs, n_tp, EARLY_QUERY, EARLY_OUT),
         out_shape=(
@@ -557,9 +651,12 @@
             pltpu.VMEM(first_moment.shape, wide),
             pltpu.VMEM(first_moment.shape, wide),
         ),
-        in_specs=[anywhere] * 6 + [vmem] * 3,
+        in_specs=[anywhere] * 10,
         out_specs=(vmem,) * 6,
         scratch_shapes=[
+            pltpu.VMEM((2, part, width), low),
+            pltpu.VMEM(first_moment.shape, wide),
+            pltpu.VMEM(first_moment.shape, wide),
             pltpu.VMEM((2, rank, model), low),
             pltpu.VMEM((2, rank, width), low),
             pltpu.VMEM((2, rank, features), low),
@@ -579,15 +676,16 @@
             pltpu.VMEM((outer, 2, depth, features), low),
             pltpu.VMEM((2, depth, features), low),
             pltpu.VMEM((n_fs + n_tp, 8, 128), wide),
-            dma((6,)),
+            dma((10,)),
             dma((2, 2, n_tp // PAIR)),
             dma((2, 2, 2, n_tp // PAIR)),
             dma((2, 2, n_tp // PAIR)),
-            dma((2, outer, 2)),
-            dma((2, outer, 2)),
-            dma((2, n_fs + n_tp)),
-            dma((4 + 2 * pieces, 9)),
-            dma((4 + 2 * pieces, 7)),
+            dma((outer, 2)),
+            dma((outer, 2)),
+            dma((2,)),
+            dma((2, 2)),
+            dma((4 + 2 * pieces,)),
+            dma((4 + 2 * pieces, 5)),
         ],
         compiler_params=pltpu.CompilerParams(
             collective_id=0, has_side_effects=True, vmem_limit_bytes=46 * 2**20
@@ -602,7 +700,8 @@
         attn_outputs,
         query_master,
         out_master,
-        factor,
+        left_factor.T,
+        right_factor.T,
         first_moment,
         second_moment,
     )
@@ -611,7 +710,7 @@
         out_shape=tuple(jax.ShapeDtypeStruct(r.shape, r.dtype) for r in results),
         in_specs=[vmem] * len(results),
         out_specs=(anywhere,) * len(results),
-        scratch_shapes=[dma((len(results),))],
+        scratch_shapes=[dma((len(results), STORES))],
         compiler_params=pltpu.CompilerParams(vmem_limit_bytes=2**20),
         cost_estimate=pl.CostEstimate(flops=2**20, bytes_accessed=13 * 2**20, transcendentals=0),
     )(*(pltpu.with_memory_space_constraint(r, pltpu.VMEM) for r in results))

time: 154 us -> 147 us (0.955)
  Pallas kernels: 152 us -> 145 us
  other arithmetic: 1.6 us -> 0 us
    pallas_call x1, Pallas kernels: 147 us -> 141 us  [fast_body(): pl.pallas_call(functools.partial(kernel, n_fs, n_tp, EARLY_QUERY, EARLY_O...]
    another operation x1 -> x0, other arithmetic: 1.6 us -> none  [fast_body(): factor = jnp.stack([left_factor.T, right_factor.T])]
where the time goes in v3:
time: 147 us; the launch traced here: 146 us
  Pallas kernels  145 us (99%)
    pallas_call x1, Pallas kernels, fast_body(): pl.pallas_call(functools.partial(kernel, n_fs, n_tp, EARLY_QUERY, EARLY_O...  141 us
    pallas_call x1, Pallas kernels, fast_body(): pl.pallas_call(store_kernel, out_shape=tuple((jax.ShapeDtypeStruct(r.shap...  4.7 us

profile of v3, /device:TPU:0, one launch (start us, length us, event | category | flops | bytes accessed | tf_op | source)
XLA Modules:
  0.0 145.9 jit_solution(15314266893538186722)
XLA Ops:
  0.6 140.5 %shard_map.145 = (f32[384,768]{1,0:T(8,128)S(1)}, f32[768,384]{1,0:T(8,128)S(1)}, bf16[3072,768]{1,0:T(8,128)(2,1)S(1)}, bf16[768,3072]{1,0:T(8,128)(2,1)S(1)}, ...) custom-call(bf16[512,3072]{1,0:T(8,128)(2,1)} %saved_hbm.1, bf16[512,3072]{1,0:T(8,128)(2,1)} %outcot_hbm.1, ...), custom_call_target="tpu_custom_call" | custom-call | flops 3019898880 | bytes 209715200 | tf_op jit(solution)/shard_map/pallas_call | solution.py:644
  141.2 4.7 %shard_map.146 = (f32[384,768]{1,0:T(8,128)}, f32[768,384]{1,0:T(8,128)}, bf16[3072,768]{1,0:T(8,128)(2,1)}, bf16[768,3072]{1,0:T(8,128)(2,1)}, f32[2,48,768]{2,1,0:T(8,128)}, /*index=5*/f32[2,48,768]{2,1,0:T(8,128)}) custom-call(f32[384,768]{1,0:T(8,128)S(1)} %get-tuple-element.12.refs_0_, f32[768,384]{1,0:T(8,128)S(1)} %get-tuple-element.13.refs_1_, ...), custom_call_target="tpu_custom_call" | custom-call | flops 1048576 | bytes 13631488 | tf_op jit(solution)/shard_map/pallas_call | solution.py:708

commit v4 on v3

--- a/solution.py
+++ b/solution.py
@@ -14,8 +14,8 @@
 EARLY_QUERY = 1
 EARLY_OUT = 1
 STORES = 4
-QUERY_ODD = (True,False,True)
-OUT_ODD = (True,False,True)
+QUERY_ODD = (True, False, True)
+OUT_ODD = (True, False, True)
 NT = (((1,), (1,)), ((), ()))
 TN = (((0,), (0,)), ((), ()))
 
@@ -367,6 +367,9 @@
         gather.launch_skew()
         gather.launch_near()
         gather.launch_cross()
+    for gather in early_o:
+        gather.launch_pair()
+        gather.launch_near()
     own_columns.forward()
 
     gathers = []
@@ -492,11 +495,6 @@
     for gather in dirs:
         gather.launch()
     dirs_ref[:, rows(me, depth), :] = own_dir[...]
-    square_all(0, n_fs - 1, 0).wait_recv()
-    mine = jnp.sum(square_buf[:n_fs], axis=0)
-    square_buf[n_fs] = mine
-    for i, peer in enumerate(tp_peers):
-        square_copy(n_fs, n_fs + 1 + i, 1, 1, peer).start()
     for gather in dirs:
         gather.relay()
     for gather in dirs:
@@ -505,12 +503,17 @@
         gather.pass_near()
         gather.pass_pair()
     for gather in early_o:
+        gather.pass_pair()
+    for gather in early_o:
         gather.launch_skew()
         gather.launch_cross()
+    square_all(0, n_fs - 1, 0).wait_recv()
+    mine = jnp.sum(square_buf[:n_fs], axis=0)
+    square_buf[n_fs] = mine
+    for i, peer in enumerate(tp_peers):
+        square_copy(n_fs, n_fs + 1 + i, 1, 1, peer).start()
     for gather in dirs:
         gather.pass_cross()
-    for gather in early_o:
-        gather.launch_pair()
     square_all(n_fs, n_tp - 1, 1).wait_recv()
     mine = jnp.sum(square_buf[n_fs:], axis=0)
     entries = dirs_ref.shape[1] * dirs_ref.shape[2] * n_tp
@@ -546,18 +549,19 @@
     bulk = early_o + late_q + late_o
 
     def finish_near(gather):
-        if gather.odd:
-            gather.launch_near()
-        gather.pass_pair()
+        if gather not in early_o:
+            if gather.odd:
+                gather.launch_near()
+            gather.pass_pair()
 
     crossing = early_q + bulk
     for i, gather in enumerate(bulk):
         gather.relay()
         if i >= 1:
             pl.when(place.end)(crossing[i + 1 - 2].pass_cross)
-        if i >= 3:
-            finish_near(bulk[i - 3])
-    for gather in bulk[max(len(bulk) - 3, 0) :]:
+        if i >= 9:
+            finish_near(bulk[i - 9])
+    for gather in bulk[max(len(bulk) - 9, 0) :]:
         finish_near(gather)
     for gather in crossing[:-2]:
         pl.when(place.inner)(gather.pass_cross)

time: 147 us -> 144 us (0.980)
  Pallas kernels: 145 us -> 143 us
    pallas_call x1, Pallas kernels: 141 us -> 138 us  [fast_body(): pl.pallas_call(functools.partial(kernel, n_fs, n_tp, EARLY_QUERY, EARLY_O...]
where the time goes in v4:
time: 144 us; the launch traced here: 143 us
  Pallas kernels  143 us (99%)
    pallas_call x1, Pallas kernels, fast_body(): pl.pallas_call(functools.partial(kernel, n_fs, n_tp, EARLY_QUERY, EARLY_O...  138 us
    pallas_call x1, Pallas kernels, fast_body(): pl.pallas_call(store_kernel, out_shape=tuple((jax.ShapeDtypeStruct(r.shap...  4.7 us

profile of v4, /device:TPU:0, one launch (start us, length us, event | category | flops | bytes accessed | tf_op | source)
XLA Modules:
  0.0 143.5 jit_solution(14480646016922632588)
XLA Ops:
  0.6 138.1 %shard_map.145 = (f32[384,768]{1,0:T(8,128)S(1)}, f32[768,384]{1,0:T(8,128)S(1)}, bf16[3072,768]{1,0:T(8,128)(2,1)S(1)}, bf16[768,3072]{1,0:T(8,128)(2,1)S(1)}, ...) custom-call(bf16[512,3072]{1,0:T(8,128)(2,1)} %saved_hbm.1, bf16[512,3072]{1,0:T(8,128)(2,1)} %outcot_hbm.1, ...), custom_call_target="tpu_custom_call" | custom-call | flops 3019898880 | bytes 209715200 | tf_op jit(solution)/shard_map/pallas_call | solution.py:648
  138.8 4.7 %shard_map.146 = (f32[384,768]{1,0:T(8,128)}, f32[768,384]{1,0:T(8,128)}, bf16[3072,768]{1,0:T(8,128)(2,1)}, bf16[768,3072]{1,0:T(8,128)(2,1)}, f32[2,48,768]{2,1,0:T(8,128)}, /*index=5*/f32[2,48,768]{2,1,0:T(8,128)}) custom-call(f32[384,768]{1,0:T(8,128)S(1)} %get-tuple-element.12.refs_0_, f32[768,384]{1,0:T(8,128)S(1)} %get-tuple-element.13.refs_1_, ...), custom_call_target="tpu_custom_call" | custom-call | flops 1048576 | bytes 13631488 | tf_op jit(solution)/shard_map/pallas_call | solution.py:712

commit v5 on v4

--- a/solution.py
+++ b/solution.py
@@ -14,6 +14,8 @@
 EARLY_QUERY = 1
 EARLY_OUT = 1
 STORES = 4
+FACTOR_CUTS = 1
+DIRECTION_CUTS = 2
 QUERY_ODD = (True, False, True)
 OUT_ODD = (True, False, True)
 NT = (((1,), (1,)), ((), ()))
@@ -294,41 +296,66 @@
             )
         )
     ]
-    for load in loads[8:] + loads[:8]:
-        load.start()
 
     fs_peers = [(lax.rem(me + i, n_fs), column) for i in range(1, n_fs)]
     tp_peers = [(me, lax.rem(column + i, n_tp)) for i in range(1, n_tp)]
     barrier = pltpu.get_barrier_semaphore()
     for peer in fs_peers + tp_peers:
         pl.semaphore_signal(barrier, inc=1, device_id=peer, device_id_type=MESH)
+    for load in loads[8:] + loads[4:8] + loads[:4]:
+        load.start()
     for load in loads[8:]:
         load.wait()
     pl.semaphore_wait(barrier, len(fs_peers) + len(tp_peers))
 
+    def launch_all(gathers):
+        for gather in gathers:
+            gather.launch_pair()
+        for gather in gathers:
+            gather.launch_skew()
+            if not gather.odd:
+                gather.launch_near()
+        for gather in gathers:
+            gather.launch_cross()
+            if gather.odd:
+                gather.launch_near()
+
     def spread(slot, view, span, odd, own=None):
         return Spread(place, view, span, spread_sends.at[slot], spread_recvs.at[slot], odd, own)
 
-    factors = [
-        spread(
-            k,
-            lambda i, k=k: factors_ref.at[k, rows(column, part), rows(i, width)],
-            lambda n, k=k: factors_ref.at[k, :part, : n * width],
-            k == 1,
-            factor_ref.at[k],
-        )
-        for k in range(2)
-    ]
-    for gather in factors:
-        gather.launch()
+    def factor_piece(k, c):
+        band = part // FACTOR_CUTS
+        start = pl.multiple_of(column * part + c * band, 16)
+        return spread(
+            k * FACTOR_CUTS + c,
+            lambda i: factors_ref.at[k, pl.ds(start, band), rows(i, width)],
+            lambda n: factors_ref.at[k, :band, : n * width],
+            (k * FACTOR_CUTS + c) % 2 == 1,
+            factor_ref.at[k, c * band : (c + 1) * band],
+        )
+
+    def direction_piece(k, c):
+        band = features // DIRECTION_CUTS
+        return spread(
+            2 * FACTOR_CUTS + k * DIRECTION_CUTS + c,
+            lambda i: dirs_ref.at[k, rows(i, depth), c * band : (c + 1) * band],
+            lambda n: dirs_ref.at[k, : n * depth, :band],
+            (k * DIRECTION_CUTS + c) % 2 == 1,
+            own_dir.at[k, :, c * band : (c + 1) * band],
+        )
+
+    factors = [factor_piece(k, c) for k in range(2) for c in range(FACTOR_CUTS)]
+    launch_all(factors)
     own_columns = Gather("tp", n_tp, lambda i: own_rows.at[:, rows(i, part), :], rows_sems, own=factor_ref)
     own_columns.start()
     factors_ref[:, rows(column, part), rows(me, width)] = factor_ref[...]
     own_rows[:, rows(column, part), :] = factor_ref[...]
 
+    first_bulk = 2 * (FACTOR_CUTS + DIRECTION_CUTS)
+
     def query_piece(i, own=None):
         return spread(
-            4 + i,
+            first_bulk + i,
             lambda j: query_copy.at[pl.ds(pl.multiple_of(j * width + i * tall, tall), tall), :],
             lambda n: query_copy.at[: n * tall, :],
             QUERY_ODD[i % 3],
@@ -337,7 +364,7 @@
 
     def out_piece(i, own=None):
         return spread(
-            4 + pieces + i,
+            first_bulk + pieces + i,
             lambda j: out_copy.at[i * deep : (i + 1) * deep, rows(j, width)],
             lambda n: out_copy.at[:deep, : n * width],
             OUT_ODD[i % 3],
@@ -355,8 +382,6 @@
     loads[5].wait()
     for i in range(early_out):
         out_early[i] = out_master[i * deep : (i + 1) * deep, :].astype(out_early.dtype)
-    for gather in early_q:
-        gather.launch_pair()
     for gather in factors:
         gather.relay()
     for gather in factors:
@@ -372,16 +397,31 @@
         gather.launch_near()
     own_columns.forward()
 
+    def project(k, tokens, origins):
+        total = None
+        for origin in origins:
+            product = lax.dot_general(
+                factors_ref[k, rows(column, part), rows(origin, width)],
+                tokens[:, rows(origin, width)],
+                NT,
+                preferred_element_type=jnp.float32,
+            )
+            total = product if total is None else total + product
+        return total
+
+    first_origins = (me, place.same(place.skew), place.same(place.cross), place.other(place.z))
+    last_origins = (place.same(place.near),) + tuple(
+        place.other(z) for z in (place.skew, place.near, place.cross)
+    )
+    first_proj = []
+    for k, tokens in enumerate((saved, outcot)):
+        loads[k].wait()
+        first_proj.append(project(k, tokens, first_origins))
     gathers = []
     for k, tokens in enumerate((saved, outcot)):
-        factors[k].collect()
-        loads[k].wait()
-        part_proj = lax.dot_general(
-            factors_ref[k, rows(column, part), :],
-            tokens[...],
-            NT,
-            preferred_element_type=jnp.float32,
-        )
+        for gather in factors[k * FACTOR_CUTS : (k + 1) * FACTOR_CUTS]:
+            gather.collect()
+        part_proj = first_proj[k] + project(k, tokens, last_origins)
         proj[k, rows(column, part), :] = part_proj.astype(proj.dtype)
         gather = Gather(
             "tp", n_tp, lambda i, k=k: proj.at[k, rows(i, part), :], proj_sems.at[k]
@@ -482,18 +522,10 @@
     square_buf[0] = mine
     for i, peer in enumerate(fs_peers):
         square_copy(0, 1 + i, 0, 1, peer).start()
-    dirs = [
-        spread(
-            2 + k,
-            lambda i, k=k: dirs_ref.at[k, rows(i, depth), :],
-            lambda n, k=k: dirs_ref.at[k, : n * depth, :],
-            k == 1,
-            own_dir.at[k],
-        )
-        for k in range(2)
-    ]
-    for gather in dirs:
-        gather.launch()
+    dirs = [direction_piece(k, c) for k in range(2) for c in range(DIRECTION_CUTS)]
+    launch_all(dirs)
+    for gather in early_q:
+        gather.launch_pair()
     dirs_ref[:, rows(me, depth), :] = own_dir[...]
     for gather in dirs:
         gather.relay()
@@ -641,6 +673,7 @@
     rank = part * n_tp
     outer = n_fs // PAIR
     pieces = width // LANES
+    slots = 2 * (FACTOR_CUTS + DIRECTION_CUTS + pieces)
     low, wide = jnp.bfloat16, jnp.float32
     vmem = pl.BlockSpec(memory_space=pltpu.VMEM)
     anywhere = pl.BlockSpec(memory_space=pl.ANY)
@@ -688,8 +721,8 @@
             dma((outer, 2)),
             dma((2,)),
             dma((2, 2)),
-            dma((4 + 2 * pieces,)),
-            dma((4 + 2 * pieces, 5)),
+            dma((slots,)),
+            dma((slots, 5)),
         ],
         compiler_params=pltpu.CompilerParams(
             collective_id=0, has_side_effects=True, vmem_limit_bytes=46 * 2**20
@@ -777,8 +810,8 @@
 def choose_body(n_fs, n_tp, *args):
     left_factor, first_moment = args[4], args[8]
     model, part = args[0].shape[1], left_factor.shape[1]
-    aligned = part % 16 == 0 and first_moment.shape[1] % 16 == 0
-    aligned = aligned and model // n_fs % 128 == 0 and first_moment.shape[2] % 256 == 0
+    aligned = part % (16 * FACTOR_CUTS) == 0 and first_moment.shape[1] % 16 == 0
+    aligned = aligned and model // n_fs % 128 == 0 and first_moment.shape[2] % (128 * DIRECTION_CUTS) == 0
     aligned = aligned and first_moment.shape[2] % (model // n_fs) == 0
     if aligned and n_fs == PAIR * LINE and n_tp % PAIR == 0:
         return fast_body(n_fs, n_tp, *args)

time: 144 us -> 141 us (0.979)
  Pallas kernels: 143 us -> 140 us
    pallas_call x1, Pallas kernels: 138 us -> 136 us  [fast_body(): pl.pallas_call(functools.partial(kernel, n_fs, n_tp, EARLY_QUERY, EARLY_O...]
where the time goes in v5:
time: 141 us
  Pallas kernels  140 us (99%)
    pallas_call x1, Pallas kernels, fast_body(): pl.pallas_call(functools.partial(kernel, n_fs, n_tp, EARLY_QUERY, EARLY_O...  136 us
    pallas_call x1, Pallas kernels, fast_body(): pl.pallas_call(store_kernel, out_shape=tuple((jax.ShapeDtypeStruct(r.shap...  4.7 us

profile of v5, /device:TPU:0, one launch (start us, length us, event | category | flops | bytes accessed | tf_op | source)
XLA Modules:
  0.0 141.1 jit_solution(5935897214689018727)
XLA Ops:
  0.6 135.8 %shard_map.145 = (f32[384,768]{1,0:T(8,128)S(1)}, f32[768,384]{1,0:T(8,128)S(1)}, bf16[3072,768]{1,0:T(8,128)(2,1)S(1)}, bf16[768,3072]{1,0:T(8,128)(2,1)S(1)}, ...) custom-call(bf16[512,3072]{1,0:T(8,128)(2,1)} %saved_hbm.1, bf16[512,3072]{1,0:T(8,128)(2,1)} %outcot_hbm.1, ...), custom_call_target="tpu_custom_call" | custom-call | flops 3019898880 | bytes 209715200 | tf_op jit(solution)/shard_map/pallas_call | solution.py:681
  136.4 4.7 %shard_map.146 = (f32[384,768]{1,0:T(8,128)}, f32[768,384]{1,0:T(8,128)}, bf16[3072,768]{1,0:T(8,128)(2,1)}, bf16[768,3072]{1,0:T(8,128)(2,1)}, f32[2,48,768]{2,1,0:T(8,128)}, /*index=5*/f32[2,48,768]{2,1,0:T(8,128)}) custom-call(f32[384,768]{1,0:T(8,128)S(1)} %get-tuple-element.12.refs_0_, f32[768,384]{1,0:T(8,128)S(1)} %get-tuple-element.13.refs_1_, ...), custom_call_target="tpu_custom_call" | custom-call | flops 1048576 | bytes 13631488 | tf_op jit(solution)/shard_map/pallas_call | solution.py:745

commit v6 on v5

--- a/solution.py
+++ b/solution.py
@@ -13,7 +13,7 @@
 LANES = 128
 EARLY_QUERY = 1
 EARLY_OUT = 1
-STORES = 4
+STORES = 1
 FACTOR_CUTS = 1
 DIRECTION_CUTS = 2
 QUERY_ODD = (True, False, True)

time: 141 us -> 141 us (level)
  no operation moved by 1% of the time
where the time goes in v6:
time: 141 us
  Pallas kernels  140 us (99%)
    pallas_call x1, Pallas kernels, fast_body(): pl.pallas_call(functools.partial(kernel, n_fs, n_tp, EARLY_QUERY, EARLY_O...  136 us
    pallas_call x1, Pallas kernels, fast_body(): pl.pallas_call(store_kernel, out_shape=tuple((jax.ShapeDtypeStruct(r.shap...  4.61 us

profile of v6, /device:TPU:0, one launch (start us, length us, event | category | flops | bytes accessed | tf_op | source)
XLA Modules:
  0.0 141.0 jit_solution(16302353023352642290)
XLA Ops:
  0.6 135.8 %shard_map.145 = (f32[384,768]{1,0:T(8,128)S(1)}, f32[768,384]{1,0:T(8,128)S(1)}, bf16[3072,768]{1,0:T(8,128)(2,1)S(1)}, bf16[768,3072]{1,0:T(8,128)(2,1)S(1)}, ...) custom-call(bf16[512,3072]{1,0:T(8,128)(2,1)} %saved_hbm.1, bf16[512,3072]{1,0:T(8,128)(2,1)} %outcot_hbm.1, ...), custom_call_target="tpu_custom_call" | custom-call | flops 3019898880 | bytes 209715200 | tf_op jit(solution)/shard_map/pallas_call | solution.py:681
  136.4 4.6 %shard_map.146 = (f32[384,768]{1,0:T(8,128)}, f32[768,384]{1,0:T(8,128)}, bf16[3072,768]{1,0:T(8,128)(2,1)}, bf16[768,3072]{1,0:T(8,128)(2,1)}, f32[2,48,768]{2,1,0:T(8,128)}, /*index=5*/f32[2,48,768]{2,1,0:T(8,128)}) custom-call(f32[384,768]{1,0:T(8,128)S(1)} %get-tuple-element.12.refs_0_, f32[768,384]{1,0:T(8,128)S(1)} %get-tuple-element.13.refs_1_, ...), custom_call_target="tpu_custom_call" | custom-call | flops 1048576 | bytes 13631488 | tf_op jit(solution)/shard_map/pallas_call | solution.py:745
